TPU v7x, 1024 devices: a whole 8x8x8 slice. The times are simulated.
1024 devices in a mesh: ep: 64 (over z, y), tp: 16 (over x, core).
Axes of the slice: x: 8, y: 8, z: 8, core: 2. Of those that a mesh axis runs over, the one named last changes fastest.
Arguments:
- tokens: bfloat16 [1024, 4096], P('ep'), may hold values from -6 to 6
- norm_gain: float32 [4096], replicated, may hold values from 0.1 to 1.9
- token_expert_index: int32 [1024, 4], P('ep'), may hold values from 0 to 63, as said below
- group_prob: float32 [1024], P('ep'), may hold values from 0.25 to 1
- expert_weight: float32 [1024, 4], P('ep'), may hold values from 0.05 to 1
- w_gate: bfloat16 [64, 4096, 2048], P('ep', None, 'tp'), may hold values from -0.09375 to 0.09375
- w_up: bfloat16 [64, 4096, 2048], P('ep', None, 'tp'), may hold values from -0.09375 to 0.09375
- w_down: bfloat16 [64, 2048, 4096], P('ep', 'tp'), may hold values from -0.125 to 0.125
Outputs:
- mixed: bfloat16 [1024, 4096], P('ep', 'tp')
Inputs may be any that keep to these rules, and one draw needn't show every extreme that they name: `token_expert_index`: each row names 4 different experts, all of one group: the group g holds experts g * 32 to (g + 1) * 32 - 1. The 16 rows of one index of ep name any one expert at most 3 times.
All inputs are finite; a program needn't handle non-finite values.
Results may differ from a plain program's by a relative error of at most 0.019.
Values may be sent and summed in bfloat16 or wider, within the bound.
No kernel may reach another device: no remote copies, remote signals or barrier semaphores. Data moves between devices by JAX's collectives and lax.ppermute only.
A program may use at most 32 MiB of HBM per device.

v0:
```python
import jax
import jax.numpy as jnp
from jax import lax
from jax.sharding import PartitionSpec as P

GROUPS = 2


def joined_along(blocks, dim):
    shape = list(blocks.shape[1:])
    shape[dim] *= blocks.shape[0]
    return jnp.moveaxis(blocks, 0, dim).reshape(shape)


def copy_for_each(x, axis):
    copies = jnp.broadcast_to(x, (lax.axis_size(axis), *x.shape))
    return lax.all_to_all(copies, axis, split_axis=0, concat_axis=0, tiled=True)


def gathered_copies(x, axis, dim):
    return joined_along(copy_for_each(x, axis), dim)


def in_blocks(x, dim, size):
    before, after = (x.shape[:dim], x.shape[dim + 1 :])
    return jnp.moveaxis(x.reshape(*before, size, -1, *after), dim, 0)


def sum_at_owner(x, axis, dim):
    blocks = in_blocks(x, dim, lax.axis_size(axis))
    arrived = lax.all_to_all(blocks, axis, split_axis=0, concat_axis=0, tiled=True)
    return arrived.astype(jnp.float32).sum(axis=0)


def body(tokens, norm_gain, token_expert_index, group_prob, expert_weight, w_gate, w_up, w_down):
    rows_here, width = tokens.shape
    topk = token_expert_index.shape[1]
    experts = lax.axis_size("ep")
    tp_count = lax.axis_size("tp")
    per_group = experts // GROUPS
    capacity = min(rows_here, max(2, rows_here * topk // max(per_group - topk, 1) + 1))
    xf = tokens.astype(jnp.float32)
    normed = (xf * lax.rsqrt(jnp.mean(xf * xf, axis=-1, keepdims=True) + 1e-06) * norm_gain).astype(
        jnp.bfloat16
    )
    gates = group_prob[:, None] * expert_weight / jnp.sum(expert_weight, axis=-1, keepdims=True)
    flattened_index = token_expert_index.reshape(-1)
    onehot = (flattened_index[:, None] == jnp.arange(experts, dtype=jnp.int32)[None, :]).astype(
        jnp.int32
    )
    earlier = jnp.cumsum(onehot, axis=0) - onehot
    slot_rank = jnp.sum(earlier * onehot, axis=1)
    place = flattened_index * capacity + slot_rank
    slots_total = experts * capacity
    select = (jnp.arange(slots_total, dtype=jnp.int32)[:, None] == place[None, :]).astype(
        jnp.float32
    )
    select = jnp.sum(select.reshape(slots_total, rows_here, topk), axis=2).astype(jnp.bfloat16)
    outgoing = jnp.dot(select, normed, preferred_element_type=jnp.float32).astype(jnp.bfloat16)
    tp_index = lax.axis_index("tp")
    share = width // tp_count
    piece = lax.dynamic_slice_in_dim(outgoing, tp_index * share, share, 1)
    arrived = lax.all_to_all(piece, "ep", split_axis=0, concat_axis=0, tiled=True)
    arrived = gathered_copies(arrived, "tp", 1)
    gate = jnp.dot(arrived, w_gate[0], preferred_element_type=jnp.float32)
    upper = jnp.dot(arrived, w_up[0], preferred_element_type=jnp.float32)
    hidden = (jax.nn.silu(gate) * upper).astype(jnp.bfloat16)
    partial_out = jnp.dot(hidden, w_down[0], preferred_element_type=jnp.float32)
    mine = sum_at_owner(partial_out.astype(jnp.bfloat16), "tp", 1).astype(jnp.bfloat16)
    returned = lax.all_to_all(mine, "ep", split_axis=0, concat_axis=0, tiled=True)
    picked = returned[place].astype(jnp.float32).reshape(rows_here, topk, share)
    mixed = jnp.sum(picked * gates[:, :, None], axis=1)
    return mixed.astype(jnp.bfloat16)


def solution(mesh):
    return jax.shard_map(
        body,
        mesh=mesh,
        in_specs=(
            P("ep", None),
            P(),
            P("ep", None),
            P("ep"),
            P("ep", None),
            P("ep", None, "tp"),
            P("ep", None, "tp"),
            P("ep", "tp", None),
        ),
        out_specs=P("ep", "tp"),
        check_vma=False,
    )
```

profile of v0, /device:TPU:1, one launch (start us, length us, event | category | flops | bytes accessed | tf_op | source)
XLA Modules:
  0.0 157.3 jit_solution(12156578799854653056)
XLA Ops:
  0.0 0.8 copy.20
  0.8 0.1 eq.30
  1.0 0.1 reduce_window_sum.11
  1.1 0.2 select_reduce_fusion
  1.5 0.1 convert_reduce_fusion
  1.6 1.1 fusion.6
  2.6 1.5 fusion.9
  4.3 35.3 %all_to_all.34 = bf16[64,3,256]{2,1,0:T(4,128)(2,1)S(1)} all-to-all(bf16[64,3,256]{2,1,0:T(4,128)(2,1)S(1)} %all_to_all.22), channel_id=1, replica_groups=mesh['ep'=64,'tp'=16] {'ep'}, dimensions={0} | all-to-all | bytes 196608 | tf_op jit(solution)/shard_map/all_to_all | solution.py:63
  39.6 0.1 broadcast_in_dim.2
  39.8 48.4 %all_to_all.35 = bf16[16,192,256]{2,1,0:T(8,128)(2,1)S(1)} all-to-all(bf16[16,192,256]{2,1,0:T(8,128)(2,1)S(1)} %broadcast_in_dim.2), channel_id=1, replica_groups=mesh['ep'=64,'tp'=16] {'tp'}, dimensions={0} | all-to-all | bytes 3145728 | tf_op jit(solution)/shard_map/all_to_all | solution.py:17
  88.1 0.2 copy.27
  88.3 1.0 copy-done.1
  89.4 0.6 fusion.4
  90.0 3.4 %convolution_convert_fusion = bf16[192,4096]{1,0:T(8,128)(2,1)} fusion(bf16[192,4096]{1,0:T(8,128)(2,1)S(1)} %bitcast.30, bf16[1,128,4096]{2,1,0:T(8,128)(2,1)S(1)} %copy-done, bf16[1,4096,128]{2,1,0:T(8,128)(2,1)} %param.14, f32[192,128]{1,0:T(8,128)S(1)} %fusion.4), kind=kOutput, calls=%fused_computation.1 | convolution fusion | flops 403587072 | bytes 5341184 | tf_op jit(solution)/shard_map/dot_general | solution.py:68
  93.4 2.7 %copy.29 = bf16[24,16,8,256]{3,2,0,1:T(8,128)(2,1)} copy(bf16[24,16,8,256]{3,2,1,0:T(8,128)(2,1)} %bitcast.33) | data formatting | bytes 3145728 | tf_op jit(solution)/shard_map/reshape | solution.py:26
  96.1 3.7 %all-to-all-start.2 = ((bf16[16,192,256]{2,1,0:T(8,128)(2,1)}), bf16[16,192,256]{2,1,0:T(8,128)(2,1)S(1)}, u32[]{:S(2)}, u32[]{:S(2)}) async-start(bf16[16,192,256]{2,1,0:T(8,128)(2,1)} %bitcast.31), calls=%async_computation.2 | async-start | bytes 3145728 | tf_op jit(solution)/shard_map/all_to_all | solution.py:31
  99.9 0.1 mul.79
  100.0 37.7 %all-to-all-done.2 = bf16[16,192,256]{2,1,0:T(8,128)(2,1)S(1)} async-done(((bf16[16,192,256]{2,1,0:T(8,128)(2,1)}), bf16[16,192,256]{2,1,0:T(8,128)(2,1)S(1)}, u32[]{:S(2)}, u32[]{:S(2)}) %all-to-all-start.2) | async-done | bytes 1572896 | tf_op jit(solution)/shard_map/all_to_all | solution.py:31
  137.7 0.2 reduce_sum.65
  137.9 0.7 all_to_all.27
  138.6 4.6 %all-to-all-start.3 = ((bf16[64,3,256]{2,1,0:T(4,128)(2,1)}), bf16[64,3,256]{2,1,0:T(4,128)(2,1)S(1)}, u32[]{:S(2)}, u32[]{:S(2)}) async-start(bf16[64,3,256]{2,1,0:T(4,128)(2,1)} %all_to_all.27), calls=%async_computation.3 | async-start | bytes 262144 | tf_op jit(solution)/shard_map/all_to_all | solution.py:70
  143.3 12.4 %all-to-all-done.3 = bf16[64,3,256]{2,1,0:T(4,128)(2,1)S(1)} async-done(((bf16[64,3,256]{2,1,0:T(4,128)(2,1)}), bf16[64,3,256]{2,1,0:T(4,128)(2,1)S(1)}, u32[]{:S(2)}, u32[]{:S(2)}) %all-to-all-start.3) | async-done | bytes 98336 | tf_op jit(solution)/shard_map/all_to_all | solution.py:70
  155.9 0.7 gather_fusion
  156.6 0.7 multiply_reduce_fusion
  (22 shorter events, 0.7 us)
Async XLA Ops:
  0.0 90.0 %copy-start = (bf16[1,128,4096]{2,1,0:T(8,128)(2,1)S(1)}, bf16[1,128,4096]{2,1,0:T(8,128)(2,1)}, u32[]{:S(2)}) copy-start(bf16[1,128,4096]{2,1,0:T(8,128)(2,1)} %param.15) | copy-start | bytes 3145732
  88.1 1.2 copy-start.1
  96.1 3.8 %copy-start.2 = (f32[16,4]{0,1:T(4,128)S(1)}, f32[16,4]{0,1:T(4,128)}, u32[]{:S(2)}) copy-start(f32[16,4]{0,1:T(4,128)} %param.12) | copy-start | bytes 772
  96.1 3.9 %copy-start.3 = (f32[16]{0:T(128)S(1)}, f32[16]{0:T(128)}, u32[]{:S(2)}) copy-start(f32[16]{0:T(128)} %param.11) | copy-start | bytes 196
  96.1 41.6 %all-to-all-start.2 = ((bf16[16,192,256]{2,1,0:T(8,128)(2,1)}), bf16[16,192,256]{2,1,0:T(8,128)(2,1)S(1)}, u32[]{:S(2)}, u32[]{:S(2)}) async-start(bf16[16,192,256]{2,1,0:T(8,128)(2,1)} %bitcast.31), calls=%async_computation.2 | async-start | bytes 3145728 | tf_op jit(solution)/shard_map/all_to_all | solution.py:31
  138.6 17.2 %all-to-all-start.3 = ((bf16[64,3,256]{2,1,0:T(4,128)(2,1)}), bf16[64,3,256]{2,1,0:T(4,128)(2,1)S(1)}, u32[]{:S(2)}, u32[]{:S(2)}) async-start(bf16[64,3,256]{2,1,0:T(4,128)(2,1)} %all_to_all.27), calls=%async_computation.3 | async-start | bytes 262144 | tf_op jit(solution)/shard_map/all_to_all | solution.py:70
where the time goes:
time: 158 us; the launch traced here: 157 us
  blocking collectives  83.6 us (53%)
  waiting for transfers between devices  50.1 us (32%)
  starting transfers between devices  8.35 us (5%)
  local copies, waits for them, and re-layouts  6.99 us (4%)
  matrix products  5.55 us (4%)
  other arithmetic  2.49 us (2%)
    all_to_all x1, blocking collectives, copy_for_each(): return lax.all_to_all(copies, axis, split_axis=0, concat_axis=0, tiled=True)  48.4 us
    all_to_all x1, waiting for transfers between devices, sum_at_owner(): lax.all_to_all(blocks, axis, split_axis=0, concat_axis=0, tiled=True)  37.7 us
    all_to_all x1, blocking collectives, body(): lax.all_to_all(piece, 'ep', split_axis=0, concat_axis=0, tiled=True)  35.3 us
    all_to_all x1, waiting for transfers between devices, body(): lax.all_to_all(mine, 'ep', split_axis=0, concat_axis=0, tiled=True)  12.4 us
    all_to_all x1, starting transfers between devices, body(): lax.all_to_all(mine, 'ep', split_axis=0, concat_axis=0, tiled=True)  4.62 us
    all_to_all x1, starting transfers between devices, sum_at_owner(): lax.all_to_all(blocks, axis, split_axis=0, concat_axis=0, tiled=True)  3.74 us
    dot_general x1, matrix products, body(): partial_out = jnp.dot(hidden, w_down[0], preferred_element_type=jnp.float32)  3.44 us
  transfers between devices with their start and end apart: 2, of which 2 were waited for; matrix products, arithmetic and copies ran while one was open for 0% of the time, Pallas kernels for 0%

commit v1 on v0

--- a/solution.py
+++ b/solution.py
@@ -12,24 +12,9 @@
     return jnp.moveaxis(blocks, 0, dim).reshape(shape)
 
 
-def copy_for_each(x, axis):
-    copies = jnp.broadcast_to(x, (lax.axis_size(axis), *x.shape))
-    return lax.all_to_all(copies, axis, split_axis=0, concat_axis=0, tiled=True)
-
-
-def gathered_copies(x, axis, dim):
-    return joined_along(copy_for_each(x, axis), dim)
-
-
 def in_blocks(x, dim, size):
     before, after = (x.shape[:dim], x.shape[dim + 1 :])
     return jnp.moveaxis(x.reshape(*before, size, -1, *after), dim, 0)
-
-
-def sum_at_owner(x, axis, dim):
-    blocks = in_blocks(x, dim, lax.axis_size(axis))
-    arrived = lax.all_to_all(blocks, axis, split_axis=0, concat_axis=0, tiled=True)
-    return arrived.astype(jnp.float32).sum(axis=0)
 
 
 def body(tokens, norm_gain, token_expert_index, group_prob, expert_weight, w_gate, w_up, w_down):
@@ -61,12 +46,13 @@
     share = width // tp_count
     piece = lax.dynamic_slice_in_dim(outgoing, tp_index * share, share, 1)
     arrived = lax.all_to_all(piece, "ep", split_axis=0, concat_axis=0, tiled=True)
-    arrived = gathered_copies(arrived, "tp", 1)
+    arrived = joined_along(lax.all_gather(arrived, "tp", axis=0), 1)
     gate = jnp.dot(arrived, w_gate[0], preferred_element_type=jnp.float32)
     upper = jnp.dot(arrived, w_up[0], preferred_element_type=jnp.float32)
     hidden = (jax.nn.silu(gate) * upper).astype(jnp.bfloat16)
     partial_out = jnp.dot(hidden, w_down[0], preferred_element_type=jnp.float32)
-    mine = sum_at_owner(partial_out.astype(jnp.bfloat16), "tp", 1).astype(jnp.bfloat16)
+    blocks = in_blocks(partial_out.astype(jnp.bfloat16), 1, tp_count)
+    mine = lax.psum_scatter(blocks, "tp", scatter_dimension=0, tiled=False)
     returned = lax.all_to_all(mine, "ep", split_axis=0, concat_axis=0, tiled=True)
     picked = returned[place].astype(jnp.float32).reshape(rows_here, topk, share)
     mixed = jnp.sum(picked * gates[:, :, None], axis=1)

time: 158 us -> 191 us (1.21)
  the two profiles are of different devices: /device:TPU:1 before, /device:TPU:16 now
where the time goes in v1:
time: 191 us
  waiting for transfers between devices  111 us (58%)
  blocking collectives  35 us (18%)
  starting transfers between devices  14.2 us (7%)
  between operations  13.5 us (7%)
  local copies, waits for them, and re-layouts  9.41 us (5%)
  matrix products  5.55 us (3%)
  other arithmetic  2.27 us (1%)
    reduce_scatter x1, waiting for transfers between devices, body(): mine = lax.psum_scatter(blocks, 'tp', scatter_dimension=0, tiled=False)  63.2 us
    all_gather x1, waiting for transfers between devices, body(): arrived = joined_along(lax.all_gather(arrived, 'tp', axis=0), 1)  36 us
    all_to_all x1, blocking collectives, body(): lax.all_to_all(piece, 'ep', split_axis=0, concat_axis=0, tiled=True)  35 us
    all_to_all x1, starting transfers between devices, body(): lax.all_to_all(mine, 'ep', split_axis=0, concat_axis=0, tiled=True)  14.2 us
    all_to_all x1, waiting for transfers between devices, body(): lax.all_to_all(mine, 'ep', split_axis=0, concat_axis=0, tiled=True)  11.8 us
  transfers between devices with their start and end apart: 3, of which 3 were waited for; matrix products, arithmetic and copies ran while one was open for 0% of the time, Pallas kernels for 0%

profile of v1, /device:TPU:16, one launch (start us, length us, event | category | flops | bytes accessed | tf_op | source)
XLA Modules:
  0.0 191.0 jit_solution(5950762387015286314)
XLA Ops:
  6.5 0.8 copy.22
  7.4 0.1 eq.30
  7.5 0.1 reduce_window_sum.11
  7.6 0.2 select_reduce_fusion
  8.0 0.1 convert_reduce_fusion
  8.1 1.1 fusion.6
  9.2 1.5 fusion.9
  10.8 35.0 %all_to_all.21 = bf16[64,3,256]{2,1,0:T(4,128)(2,1)S(1)} all-to-all(bf16[64,3,256]{2,1,0:T(4,128)(2,1)S(1)} %all_to_all.14), channel_id=1, replica_groups=mesh['ep'=64,'tp'=16] {'ep'}, dimensions={0} | all-to-all | bytes 196608 | tf_op jit(solution)/shard_map/all_to_all | solution.py:48
  45.8 0.7 all_gather.6
  46.6 36.0 %all-gather.2.cloned.1.call-done = bf16[16,192,256]{2,1,0:T(8,128)(2,1)} async-done(((bf16[1,192,256]{2,1,0:T(8,128)(2,1)}), bf16[16,192,256]{2,1,0:T(8,128)(2,1)}) %all-gather.2.cloned.1.call-update) | async-done | bytes 1572880 | tf_op jit(solution)/shard_map/all_gather | solution.py:49
  82.6 1.7 copy.29
  84.3 0.6 fusion.4
  84.9 3.4 %convolution_convert_fusion = bf16[192,4096]{1,0:T(8,128)(2,1)} fusion(bf16[192,4096]{1,0:T(8,128)(2,1)S(1)} %bitcast.30, bf16[1,128,4096]{2,1,0:T(8,128)(2,1)S(1)} %copy-done, bf16[1,4096,128]{2,1,0:T(8,128)(2,1)} %param.14, f32[192,128]{1,0:T(8,128)S(1)} %fusion.4), kind=kOutput, calls=%fused_computation.1 | convolution fusion | flops 403587072 | bytes 5341184 | tf_op jit(solution)/shard_map/dot_general | solution.py:53
  88.3 2.7 %copy.31 = bf16[24,16,8,256]{3,2,0,1:T(8,128)(2,1)} copy(bf16[24,16,8,256]{3,2,1,0:T(8,128)(2,1)} %bitcast.32) | data formatting | bytes 3145728 | tf_op jit(solution)/shard_map/reshape | solution.py:17
  91.1 0.1 mul.79
  91.2 0.6 copy-done.2
  91.8 63.2 %reduce-scatter.2.cloned.1.call-done = bf16[1,192,256]{2,1,0:T(8,128)(2,1)} async-done(((bf16[16,192,256]{2,1,0:T(8,128)(2,1)}), bf16[1,192,256]{2,1,0:T(8,128)(2,1)}) %reduce-scatter.2.cloned.1.call-update) | async-done | bytes 98320 | tf_op jit(solution)/shard_map/reduce_scatter | solution.py:55
  155.0 1.6 all_to_all.16
  156.5 14.2 %all-to-all-start.1 = ((bf16[64,3,256]{2,1,0:T(4,128)(2,1)}), bf16[64,3,256]{2,1,0:T(4,128)(2,1)S(1)}, u32[]{:S(2)}, u32[]{:S(2)}) async-start(bf16[64,3,256]{2,1,0:T(4,128)(2,1)} %all_to_all.16), calls=%async_computation.2 | async-start | bytes 262144 | tf_op jit(solution)/shard_map/all_to_all | solution.py:56
  170.7 0.1 copy.27
  170.8 11.8 %all-to-all-done.1 = bf16[64,3,256]{2,1,0:T(4,128)(2,1)S(1)} async-done(((bf16[64,3,256]{2,1,0:T(4,128)(2,1)}), bf16[64,3,256]{2,1,0:T(4,128)(2,1)S(1)}, u32[]{:S(2)}, u32[]{:S(2)}) %all-to-all-start.1) | async-done | bytes 98336 | tf_op jit(solution)/shard_map/all_to_all | solution.py:56
  182.6 0.1 all_to_all.18
  182.7 0.7 gather_fusion
  183.4 0.7 multiply_reduce_fusion
  (23 shorter events, 0.5 us)
Async XLA Ops:
  6.5 78.4 %copy-start = (bf16[1,128,4096]{2,1,0:T(8,128)(2,1)S(1)}, bf16[1,128,4096]{2,1,0:T(8,128)(2,1)}, u32[]{:S(2)}) copy-start(bf16[1,128,4096]{2,1,0:T(8,128)(2,1)} %param.15) | copy-start | bytes 3145732
  6.5 76.1 %all-gather.2.cloned.1.call-start = ((), (), s32[]{:S(2)}) async-start(), calls=%async_computation.3 | async-start | bytes 1671168 | tf_op jit(solution)/shard_map/all_gather | solution.py:49
  46.5 108.5 %reduce-scatter.2.cloned.1.call-start = ((), (), s32[]{:S(2)}) async-start(), calls=%async_computation.4 | async-start | bytes 1671168 | tf_op jit(solution)/shard_map/reduce_scatter | solution.py:55
  82.6 1.7 copy-start.1
  91.1 0.7 copy-start.2
  91.1 0.7 copy-start.3
  156.5 26.1 %all-to-all-start.1 = ((bf16[64,3,256]{2,1,0:T(4,128)(2,1)}), bf16[64,3,256]{2,1,0:T(4,128)(2,1)S(1)}, u32[]{:S(2)}, u32[]{:S(2)}) async-start(bf16[64,3,256]{2,1,0:T(4,128)(2,1)} %all_to_all.16), calls=%async_computation.2 | async-start | bytes 262144 | tf_op jit(solution)/shard_map/all_to_all | solution.py:56
Sparse Core Ops, SparseCore 0:
  46.6 35.9 all-gather.1
  91.2 63.7 reduce-scatter.1

commit v2 on v1

v2 whole, which is shorter than its diff:
```python
import jax
import jax.numpy as jnp
from jax import lax
from jax.sharding import PartitionSpec as P

GROUPS = 2


def body(tokens, norm_gain, token_expert_index, group_prob, expert_weight, w_gate, w_up, w_down):
    rows_here, width = tokens.shape
    topk = token_expert_index.shape[1]
    experts = lax.axis_size("ep")
    tp_count = lax.axis_size("tp")
    chips = tp_count // 2
    share = width // tp_count
    half = width // 2
    core = lax.axis_index("tp") % 2
    swap = [(i, i ^ 1) for i in range(tp_count)]
    same_core = [[2 * i + c for i in range(chips)] for c in range(2)]
    per_group = experts // GROUPS
    capacity = min(rows_here, max(2, rows_here * topk // max(per_group - topk, 1) + 1))
    slots_total = experts * capacity
    xf = tokens.astype(jnp.float32)
    normed = (xf * lax.rsqrt(jnp.mean(xf * xf, axis=-1, keepdims=True) + 1e-06) * norm_gain).astype(
        jnp.bfloat16
    )
    gates = group_prob[:, None] * expert_weight / jnp.sum(expert_weight, axis=-1, keepdims=True)
    flattened_index = token_expert_index.reshape(-1)
    onehot = (flattened_index[:, None] == jnp.arange(experts, dtype=jnp.int32)[None, :]).astype(
        jnp.int32
    )
    earlier = jnp.cumsum(onehot, axis=0) - onehot
    slot_rank = jnp.sum(earlier * onehot, axis=1)
    place = flattened_index * capacity + slot_rank
    at_place = jnp.arange(slots_total, dtype=jnp.int32)[:, None] == place[None, :]
    select = jnp.sum(
        at_place.astype(jnp.float32).reshape(slots_total, rows_here, topk), axis=2
    ).astype(jnp.bfloat16)

    mine_in = lax.dynamic_slice_in_dim(normed.reshape(rows_here, chips, 2, share), core, 1, 2)
    outgoing = jnp.dot(
        select, mine_in.reshape(rows_here, half), preferred_element_type=jnp.float32
    ).astype(jnp.bfloat16)
    outgoing = outgoing.reshape(experts, capacity * chips, share)
    arrived = lax.all_to_all(outgoing, "ep", split_axis=0, concat_axis=0, tiled=True)
    other = lax.ppermute(arrived, "tp", swap)
    arrived = arrived.reshape(slots_total, half)
    other = other.reshape(slots_total, half)

    def rows_of(w, which):
        w = w.reshape(chips, 2, share, w.shape[1])
        return lax.dynamic_slice_in_dim(w, which, 1, 1).reshape(half, w.shape[3])

    def into(w):
        a = jnp.dot(arrived, rows_of(w, core), preferred_element_type=jnp.float32)
        b = jnp.dot(other, rows_of(w, 1 - core), preferred_element_type=jnp.float32)
        return a + b

    hidden = (jax.nn.silu(into(w_gate[0])) * into(w_up[0])).astype(jnp.bfloat16)

    down = w_down[0].reshape(-1, chips, 2, share)

    def out_of(which):
        w = lax.dynamic_slice_in_dim(down, which, 1, 2).reshape(-1, half)
        return jnp.dot(hidden, w, preferred_element_type=jnp.float32).astype(jnp.bfloat16)

    theirs = lax.ppermute(out_of(1 - core), "tp", swap)
    mine = (out_of(core).astype(jnp.float32) + theirs.astype(jnp.float32)).astype(jnp.bfloat16)
    mine = mine.reshape(experts, capacity * chips, share)
    returned = lax.all_to_all(mine, "ep", split_axis=0, concat_axis=0, tiled=True)
    returned = returned.reshape(slots_total, half)
    weigh = jnp.sum(
        (at_place.astype(jnp.float32) * gates.reshape(-1)[None, :]).reshape(
            slots_total, rows_here, topk
        ),
        axis=2,
    )
    partial_mix = jnp.dot(
        weigh.T,
        returned.astype(jnp.float32),
        precision=lax.Precision.HIGHEST,
        preferred_element_type=jnp.float32,
    ).astype(jnp.bfloat16)
    blocks = jnp.moveaxis(partial_mix.reshape(rows_here, chips, share), 1, 0)
    parts = lax.all_to_all(
        blocks, "tp", split_axis=0, concat_axis=0, tiled=True, axis_index_groups=same_core
    )
    return parts.astype(jnp.float32).sum(axis=0).astype(jnp.bfloat16)


def solution(mesh):
    return jax.shard_map(
        body,
        mesh=mesh,
        in_specs=(
            P("ep", None),
            P(),
            P("ep", None),
            P("ep"),
            P("ep", None),
            P("ep", None, "tp"),
            P("ep", None, "tp"),
            P("ep", "tp", None),
        ),
        out_specs=P("ep", "tp"),
        check_vma=False,
    )
```

time: 191 us -> 116 us (0.61)
  waiting for transfers between devices: 111 us -> 25.2 us
  starting transfers between devices: 14.2 us -> 27.7 us
  between operations: 13.5 us -> 0.25 us
  blocking collectives: 35 us -> 45.8 us
  matrix products: 5.55 us -> 2.95 us
    reduce_scatter x1 -> x0, waiting for transfers between devices: 63.2 us -> none  [body(): mine = lax.psum_scatter(blocks, 'tp', scatter_dimension=0, tiled=False)]
    all_gather x1 -> x0, waiting for transfers between devices: 36 us -> none  [body(): arrived = joined_along(lax.all_gather(arrived, 'tp', axis=0), 1)]
    all_to_all x1, waiting for transfers between devices: 11.8 us -> 23.3 us  [body(): lax.all_to_all(outgoing, 'ep', split_axis=0, concat_axis=0, tiled=True)]
    all_to_all x1 -> x2, blocking collectives: 35 us -> 45.8 us  [the longest x1 30.9 us: body(): lax.all_to_all(mine, 'ep', split_axis=0, concat_axis=0, tiled=True)]
    all_to_all x1, starting transfers between devices: 14.2 us -> 23.4 us  [body(): lax.all_to_all(outgoing, 'ep', split_axis=0, concat_axis=0, tiled=True)]
    ppermute x0 -> x2, starting transfers between devices: none -> 4.31 us  [the longest x1 2.4 us: body(): theirs = lax.ppermute(out_of(1 - core), 'tp', swap)]
    dot_general x3 -> x8, matrix products: 5.55 us -> 2.95 us  [the longest x2 0.73 us: out_of(): jnp.dot(hidden, w, preferred_element_type=jnp.float32).astype(jnp.bfloat16)]
    dynamic_slice x0 -> x3, local copies, waits for them, and re-layouts: none -> 2.49 us  [the longest x1 1.09 us: out_of(): w = lax.dynamic_slice_in_dim(down, which, 1, 2).reshape(-1, half)]
  transfers between devices with their start and end apart: 3 -> 3, of which waited for: 3 -> 2; matrix products, arithmetic and copies ran while one was open for 0% -> 3% of each run, Pallas kernels for 0% -> 0%
where the time goes in v2:
time: 116 us; the launch traced here: 115 us
  blocking collectives  45.8 us (39%)
  starting transfers between devices  27.7 us (24%)
  waiting for transfers between devices  25.2 us (22%)
  local copies, waits for them, and re-layouts  9.6 us (8%)
  other arithmetic  3.84 us (3%)
  matrix products  2.95 us (3%)
    all_to_all x1, blocking collectives, body(): lax.all_to_all(mine, 'ep', split_axis=0, concat_axis=0, tiled=True)  30.9 us
    all_to_all x1, starting transfers between devices, body(): lax.all_to_all(outgoing, 'ep', split_axis=0, concat_axis=0, tiled=True)  23.4 us
    all_to_all x1, waiting for transfers between devices, body(): lax.all_to_all(outgoing, 'ep', split_axis=0, concat_axis=0, tiled=True)  23.3 us
    all_to_all x1, blocking collectives, body(): lax.all_to_all(blocks, 'tp', split_axis=0, concat_axis=0, tiled=True, axi...  14.9 us
    unnamed x19, local copies, waits for them, and re-layouts  3 us
    ppermute x1, starting transfers between devices, body(): theirs = lax.ppermute(out_of(1 - core), 'tp', swap)  2.4 us
  transfers between devices with their start and end apart: 3, of which 2 were waited for; matrix products, arithmetic and copies ran while one was open for 3% of the time, Pallas kernels for 0%

profile of v2, /device:TPU:16, one launch (start us, length us, event | category | flops | bytes accessed | tf_op | source)
XLA Modules:
  0.0 115.4 jit_solution(17837377042690826849)
XLA Ops:
  0.0 0.8 copy.33
  1.4 0.7 multiply_add_fusion
  2.1 1.0 fusion.3
  3.2 1.0 fusion.5
  4.3 0.4 dynamic-slice_reduce_fusion
  4.8 0.4 convolution_convert_fusion.2
  5.2 1.2 %reshape.89 = bf16[64,24,256]{2,1,0:T(8,128)(2,1)} reshape(bf16[192,2048]{1,0:T(8,128)(2,1)S(1)} %convolution_convert_fusion.2) | data formatting | bytes 1572864 | tf_op jit(solution)/shard_map/reshape | solution.py:44
  6.5 23.4 %all-to-all-start = ((bf16[64,24,256]{2,1,0:T(8,128)(2,1)}), bf16[64,24,256]{2,1,0:T(8,128)(2,1)S(1)}, u32[]{:S(2)}, u32[]{:S(2)}) async-start(bf16[64,24,256]{2,1,0:T(8,128)(2,1)} %reshape.89), calls=%async_computation | async-start | bytes 1572864 | tf_op jit(solution)/shard_map/all_to_all | solution.py:45
  29.9 0.7 copy.36
  30.6 23.3 %all-to-all-done = bf16[64,24,256]{2,1,0:T(8,128)(2,1)S(1)} async-done(((bf16[64,24,256]{2,1,0:T(8,128)(2,1)}), bf16[64,24,256]{2,1,0:T(8,128)(2,1)S(1)}, u32[]{:S(2)}, u32[]{:S(2)}) %all-to-all-start) | async-done | bytes 786464 | tf_op jit(solution)/shard_map/all_to_all | solution.py:45
  53.9 1.9 %collective-permute-start = (bf16[64,24,256]{2,1,0:T(8,128)(2,1)S(1)}, bf16[64,24,256]{2,1,0:T(8,128)(2,1)}, u32[]{:S(2)}, u32[]{:S(2)}) collective-permute-start(bf16[64,24,256]{2,1,0:T(8,128)(2,1)S(1)} %all-to-all-done), channel_id=1, source_target_pairs={{0,1},{1,0},{2,3},{3,2},{4,5},{5,4},{6,7},{7,6},{8,9},{9,8},{10,11... | collective-permute-start | bytes 2359304 | tf_op jit(solution)/shard_map/ppermute | solution.py:46
  55.8 1.1 constant_dynamic-slice_fusion.5
  56.9 0.5 copy-done.2
  57.7 1.0 constant_dynamic-slice_fusion.1
  59.8 1.5 %reshape.92 = bf16[192,2048]{1,0:T(8,128)(2,1)S(1)} reshape(bf16[64,24,256]{2,1,0:T(8,128)(2,1)} %collective-permute-done) | data formatting | bytes 1572864 | tf_op jit(solution)/shard_map/reshape | solution.py:48
  61.7 0.7 copy-done.5
  62.7 0.4 convolution_convert_fusion
  63.1 2.4 %collective-permute-start.1 = (bf16[192,2048]{1,0:T(8,128)(2,1)S(1)}, bf16[192,2048]{1,0:T(8,128)(2,1)S(1)}, u32[]{:S(2)}, u32[]{:S(2)}) collective-permute-start(bf16[192,2048]{1,0:T(8,128)(2,1)S(1)} %convolution_convert_fusion), channel_id=1, source_target_pairs={{0,1},{1,0},{2,3},{3,2},{4,5},{5,4},{6,7},{7,6},{8,9},{9,8},{10,11... | collective-permute-start | bytes 2359304 | tf_op jit(solution)/shard_map/ppermute | solution.py:67
  65.5 1.9 %collective-permute-done.1 = bf16[192,2048]{1,0:T(8,128)(2,1)S(1)} collective-permute-done((bf16[192,2048]{1,0:T(8,128)(2,1)S(1)}, bf16[192,2048]{1,0:T(8,128)(2,1)S(1)}, u32[]{:S(2)}, u32[]{:S(2)}) %collective-permute-start.1) | collective-permute-done | bytes 786464 | tf_op jit(solution)/shard_map/ppermute | solution.py:67
  67.4 0.4 add_convert_fusion
  68.1 30.9 %all_to_all.15 = bf16[64,24,256]{2,1,0:T(8,128)(2,1)S(1)} all-to-all(bf16[64,24,256]{2,1,0:T(8,128)(2,1)S(1)} %reshape.98), channel_id=1, replica_groups=mesh['ep'=64,'tp'=16] {'ep'}, dimensions={0} | all-to-all | bytes 1572864 | tf_op jit(solution)/shard_map/all_to_all | solution.py:70
  99.4 0.4 convolution_convert_fusion.3
  99.8 14.9 %all_to_all.16 = bf16[8,16,256]{2,1,0:T(8,128)(2,1)S(1)} all-to-all(bf16[8,16,256]{2,1,0:T(8,128)(2,1)S(1)} %bitcast.44), channel_id=1, replica_groups={{0,2,4,6,8,10,12,14},{1,3,5,7,9,11,13,15},{16,18,20,22,24,26,28,30},{17..., dimensions={0} | all-to-all | bytes 131072 | tf_op jit(solution)/shard_map/all_to_all | solution.py:85
  114.8 0.6 reduce_sum.65
  (35 shorter events, 3.7 us)
Async XLA Ops:
  0.0 4.7 %copy-start.6 = (f32[16,4]{0,1:T(4,128)S(1)}, f32[16,4]{0,1:T(4,128)}, u32[]{:S(2)}) copy-start(f32[16,4]{0,1:T(4,128)} %param.12) | copy-start | bytes 772
  0.0 4.7 %copy-start.7 = (f32[16]{0:T(128)S(1)}, f32[16]{0:T(128)}, u32[]{:S(2)}) copy-start(f32[16]{0:T(128)} %param.11) | copy-start | bytes 196
  6.5 23.4 %copy-start.4 = (bf16[1,128,4096]{2,1,0:T(8,128)(2,1)S(1)}, bf16[1,128,4096]{2,1,0:T(8,128)(2,1)}, u32[]{:S(2)}) copy-start(bf16[1,128,4096]{2,1,0:T(8,128)(2,1)} %param.15) | copy-start | bytes 3145732
  6.5 47.4 %all-to-all-start = ((bf16[64,24,256]{2,1,0:T(8,128)(2,1)}), bf16[64,24,256]{2,1,0:T(8,128)(2,1)S(1)}, u32[]{:S(2)}, u32[]{:S(2)}) async-start(bf16[64,24,256]{2,1,0:T(8,128)(2,1)} %reshape.89), calls=%async_computation | async-start | bytes 1572864 | tf_op jit(solution)/shard_map/all_to_all | solution.py:45
  53.9 5.9 %collective-permute-start = (bf16[64,24,256]{2,1,0:T(8,128)(2,1)S(1)}, bf16[64,24,256]{2,1,0:T(8,128)(2,1)}, u32[]{:S(2)}, u32[]{:S(2)}) collective-permute-start(bf16[64,24,256]{2,1,0:T(8,128)(2,1)S(1)} %all-to-all-done), channel_id=1, source_target_pairs={{0,1},{1,0},{2,3},{3,2},{4,5},{5,4},{6,7},{7,6},{8,9},{9,8},{10,11... | collective-permute-start | bytes 2359304 | tf_op jit(solution)/shard_map/ppermute | solution.py:46
  55.8 1.6 %copy-start.2 = (bf16[1,4096,128]{2,1,0:T(8,128)(2,1)S(1)}, bf16[1,4096,128]{2,1,0:T(8,128)(2,1)}, u32[]{:S(2)}) copy-start(bf16[1,4096,128]{2,1,0:T(8,128)(2,1)} %param.14) | copy-start | bytes 3145732
  55.8 1.9 %copy-start.3 = (bf16[1,4096,128]{2,1,0:T(8,128)(2,1)S(1)}, bf16[1,4096,128]{2,1,0:T(8,128)(2,1)}, u32[]{:S(2)}) copy-start(bf16[1,4096,128]{2,1,0:T(8,128)(2,1)} %param.13) | copy-start | bytes 3145732
  61.3 1.0 copy-start.5
  61.6 1.1 copy-start.1
  62.7 4.7 %copy-start = (bf16[128,8,1,256]{0,3,2,1:T(8,128)(2,1)S(1)}, bf16[128,8,1,256]{0,3,2,1:T(8,128)(2,1)}, u32[]{:S(2)}) copy-start(bf16[128,8,1,256]{0,3,2,1:T(8,128)(2,1)} %get-tuple-element.8) | copy-start | bytes 1572868
  63.1 4.3 %collective-permute-start.1 = (bf16[192,2048]{1,0:T(8,128)(2,1)S(1)}, bf16[192,2048]{1,0:T(8,128)(2,1)S(1)}, u32[]{:S(2)}, u32[]{:S(2)}) collective-permute-start(bf16[192,2048]{1,0:T(8,128)(2,1)S(1)} %convolution_convert_fusion), channel_id=1, source_target_pairs={{0,1},{1,0},{2,3},{3,2},{4,5},{5,4},{6,7},{7,6},{8,9},{9,8},{10,11... | collective-permute-start | bytes 2359304 | tf_op jit(solution)/shard_map/ppermute | solution.py:67

commit v3 on v2

v3 whole, which is shorter than its diff:
```python
import jax
import jax.numpy as jnp
from jax import lax
from jax.experimental import pallas as pl
from jax.experimental.pallas import tpu as pltpu
from jax.sharding import PartitionSpec as P

GROUPS = 2
BLOCK = 256
LANES = 128


def dispatch_kernel(core_ref, index_ref, tokens_ref, gain_ref, out_ref, count_ref, *lanes):
    tokens, width = tokens_ref.shape
    experts, _, chips, share = out_ref.shape
    topk = index_ref.shape[0] // tokens
    core = core_ref[0]
    xf = tokens_ref[...].astype(jnp.float32)
    scale = lax.rsqrt(jnp.mean(xf * xf, axis=-1, keepdims=True) + 1e-06)
    for b in range(chips):
        at = pl.multiple_of((2 * b + core) * share, share)
        block = tokens_ref[:, pl.ds(at, share)].astype(jnp.float32)
        block = block * scale * gain_ref[:, pl.ds(at, share)]
        for i, ref in enumerate(lanes):
            ref[pl.ds(b, tokens, stride=chips), :] = block[:, i * LANES : (i + 1) * LANES]
    out_ref[...] = jnp.zeros_like(out_ref)

    def clear(e, _):
        count_ref[e] = 0

    lax.fori_loop(0, experts, clear, None, unroll=8)

    def token(t, _):
        here = pl.ds(pl.multiple_of(t * chips, chips), chips)
        row = jnp.concatenate([ref[here, :] for ref in lanes], axis=1).astype(jnp.bfloat16)
        for k in range(topk):
            e = index_ref[t * topk + k]
            rank = count_ref[e]
            count_ref[e] = rank + 1
            out_ref[e, rank] = row

    lax.fori_loop(0, tokens, token, None)


def block_at(b, which):
    return pl.ds(pl.multiple_of((2 * b + which) * BLOCK, BLOCK), BLOCK)


def fetch(which, sources, buffer, sems):
    copies = []
    for b in range(buffer.shape[1]):
        pair = []
        for i, source in enumerate(sources):
            pair.append(
                pltpu.make_async_copy(source.at[block_at(b, which)], buffer.at[i, b], sems.at[i, b])
            )
            pair[-1].start()
        copies.append(pair)
    return copies


def project(x_ref, copies, buffer, gate, up):
    for b, pair in enumerate(copies):
        x = x_ref[:, b * BLOCK : (b + 1) * BLOCK]
        for copy in pair:
            copy.wait()
        gate += jnp.dot(x, buffer[0, b], preferred_element_type=jnp.float32)
        up += jnp.dot(x, buffer[1, b], preferred_element_type=jnp.float32)
    return gate, up


def own_kernel(core_ref, x_ref, gate_ref, up_ref, sums_ref, buffer, sems):
    copies = fetch(core_ref[0], (gate_ref, up_ref), buffer, sems)
    zero = jnp.zeros(sums_ref.shape[1:], jnp.float32)
    sums_ref[0], sums_ref[1] = project(x_ref, copies, buffer, zero, zero)


def other_kernel(
    core_ref, x_ref, sums_ref, gate_ref, up_ref, down_ref, keep_ref, send_ref, buffer, sems, down, sem
):
    core = core_ref[0]
    copies = fetch(1 - core, (gate_ref, up_ref), buffer, sems)
    rest = pltpu.make_async_copy(down_ref, down, sem)
    rest.start()
    gate, up = project(x_ref, copies, buffer, sums_ref[0], sums_ref[1])
    hidden = (gate * jax.nn.sigmoid(gate) * up).astype(jnp.bfloat16)
    rest.wait()
    for ref, which in ((send_ref, 1 - core), (keep_ref, core)):
        for b in range(buffer.shape[1]):
            out = jnp.dot(hidden, down[:, block_at(b, which)], preferred_element_type=jnp.float32)
            ref[:, b * BLOCK : (b + 1) * BLOCK] = out.astype(jnp.bfloat16)


GRANT = pltpu.CompilerParams(vmem_limit_bytes=16 * 2**20)
SMEM = pl.BlockSpec(memory_space=pltpu.SMEM)
VMEM = pl.BlockSpec(memory_space=pltpu.VMEM)
HBM = pl.BlockSpec(memory_space=pltpu.HBM)


def in_vmem(x):
    return pltpu.with_memory_space_constraint(x, pltpu.VMEM)


def in_hbm(x):
    return pltpu.with_memory_space_constraint(x, pltpu.HBM)


def body(tokens, norm_gain, token_expert_index, group_prob, expert_weight, w_gate, w_up, w_down):
    rows_here, width = tokens.shape
    topk = token_expert_index.shape[1]
    experts = lax.axis_size("ep")
    tp_count = lax.axis_size("tp")
    chips = tp_count // 2
    share = width // tp_count
    half = width // 2
    core = lax.axis_index("tp") % 2
    swap = [(i, i ^ 1) for i in range(tp_count)]
    same_core = [[2 * i + c for i in range(chips)] for c in range(2)]
    per_group = experts // GROUPS
    capacity = min(rows_here, max(2, rows_here * topk // max(per_group - topk, 1) + 1))
    slots_total = experts * capacity
    gates = group_prob[:, None] * expert_weight / jnp.sum(expert_weight, axis=-1, keepdims=True)
    flattened_index = token_expert_index.reshape(-1)
    onehot = (flattened_index[:, None] == jnp.arange(experts, dtype=jnp.int32)[None, :]).astype(
        jnp.int32
    )
    earlier = jnp.cumsum(onehot, axis=0) - onehot
    slot_rank = jnp.sum(earlier * onehot, axis=1)
    place = flattened_index * capacity + slot_rank
    at_place = jnp.arange(slots_total, dtype=jnp.int32)[:, None] == place[None, :]
    core_id = core.astype(jnp.int32).reshape(1)
    outgoing = pl.pallas_call(
        dispatch_kernel,
        out_shape=pltpu.VMEM((experts, capacity, chips, share), jnp.bfloat16),
        in_specs=[SMEM, SMEM, VMEM, VMEM],
        out_specs=VMEM,
        scratch_shapes=[
            pltpu.SMEM((experts,), jnp.int32),
            *[pltpu.VMEM((rows_here * chips, LANES), jnp.float32)] * (share // LANES),
        ],
        compiler_params=GRANT,
        name="dispatch",
    )(core_id, flattened_index, tokens, norm_gain[None, :])
    outgoing = outgoing.reshape(experts, capacity * chips, share)
    arrived = lax.all_to_all(outgoing, "ep", split_axis=0, concat_axis=0, tiled=True)
    other = lax.ppermute(arrived, "tp", swap)
    arrived = arrived.reshape(slots_total, half)
    other = other.reshape(slots_total, half)

    units = w_gate.shape[2]
    both = pltpu.VMEM((slots_total, half), jnp.bfloat16)
    weights = [
        pltpu.VMEM((2, chips, share, units), jnp.bfloat16),
        pltpu.SemaphoreType.DMA((2, chips)),
    ]
    sums = pl.pallas_call(
        own_kernel,
        out_shape=pltpu.VMEM((2, slots_total, units), jnp.float32),
        in_specs=[SMEM, VMEM, HBM, HBM],
        out_specs=VMEM,
        scratch_shapes=weights,
        compiler_params=GRANT,
        name="own_half",
    )(core_id, in_vmem(arrived), in_hbm(w_gate[0]), in_hbm(w_up[0]))
    keep, send = pl.pallas_call(
        other_kernel,
        out_shape=(both, both),
        in_specs=[SMEM, VMEM, VMEM, HBM, HBM, HBM],
        out_specs=(VMEM, VMEM),
        scratch_shapes=weights
        + [pltpu.VMEM((units, width), jnp.bfloat16), pltpu.SemaphoreType.DMA],
        compiler_params=GRANT,
        name="other_half",
    )(core_id, in_vmem(other), in_vmem(sums), *(in_hbm(w[0]) for w in (w_gate, w_up, w_down)))
    theirs = lax.ppermute(send, "tp", swap)
    mine = (keep.astype(jnp.float32) + theirs.astype(jnp.float32)).astype(jnp.bfloat16)
    mine = mine.reshape(experts, capacity * chips, share)
    returned = lax.all_to_all(mine, "ep", split_axis=0, concat_axis=0, tiled=True)
    returned = returned.reshape(slots_total, half)
    weigh = jnp.sum(
        (at_place.astype(jnp.float32) * gates.reshape(-1)[None, :]).reshape(
            slots_total, rows_here, topk
        ),
        axis=2,
    )
    partial_mix = jnp.dot(
        weigh.T,
        returned.astype(jnp.float32),
        precision=lax.Precision.HIGHEST,
        preferred_element_type=jnp.float32,
    ).astype(jnp.bfloat16)
    blocks = jnp.moveaxis(partial_mix.reshape(rows_here, chips, share), 1, 0)
    parts = lax.all_to_all(
        blocks, "tp", split_axis=0, concat_axis=0, tiled=True, axis_index_groups=same_core
    )
    return parts.astype(jnp.float32).sum(axis=0).astype(jnp.bfloat16)


def solution(mesh):
    return jax.shard_map(
        body,
        mesh=mesh,
        in_specs=(
            P("ep", None),
            P(),
            P("ep", None),
            P("ep"),
            P("ep", None),
            P("ep", None, "tp"),
            P("ep", None, "tp"),
            P("ep", "tp", None),
        ),
        out_specs=P("ep", "tp"),
        check_vma=False,
    )
```

time: 116 us -> 113 us (0.974)
  starting transfers between devices: 27.7 us -> 11 us
  blocking collectives: 45.8 us -> 62 us
  Pallas kernels: 0 us -> 6.99 us
  local copies, waits for them, and re-layouts: 9.6 us -> 4.97 us
  matrix products: 2.95 us -> 0.42 us
  other arithmetic: 3.84 us -> 1.34 us
    all_to_all x1, starting transfers between devices: 23.4 us -> 6.64 us  [body(): lax.all_to_all(mine, 'ep', split_axis=0, concat_axis=0, tiled=True)]
    all_to_all x1, blocking collectives: 30.9 us -> 47.1 us  [body(): lax.all_to_all(outgoing, 'ep', split_axis=0, concat_axis=0, tiled=True)]
    pallas_call x0 -> x3, Pallas kernels: none -> 6.99 us  [the longest x1 3.28 us: body(): pl.pallas_call(other_kernel, out_shape=(both, both), in_specs=[SMEM, VMEM...]
    dot_general x7 -> x0, matrix products: 2.53 us -> none  [the longest x2 0.73 us: out_of(): jnp.dot(hidden, w, preferred_element_type=jnp.float32).astype(jnp.bfloat16)]
    dynamic_slice x3 -> x0, local copies, waits for them, and re-layouts: 2.49 us -> none  [the longest x1 1.09 us: out_of(): w = lax.dynamic_slice_in_dim(down, which, 1, 2).reshape(-1, half)]
    reshape x2 -> x0, local copies, waits for them, and re-layouts: 1.31 us -> none  [the longest x1 1.24 us: body(): outgoing = outgoing.reshape(experts, capacity * chips, share)]
    unnamed x19 -> x11, local copies, waits for them, and re-layouts: 3 us -> 2.38 us
  transfers between devices with their start and end apart: 3 -> 3, of which waited for: 2 -> 2; matrix products, arithmetic and copies ran while one was open for 3% -> 1% of each run, Pallas kernels for 0% -> 2%
where the time goes in v3:
time: 113 us
  blocking collectives  62 us (55%)
  waiting for transfers between devices  25.8 us (23%)
  starting transfers between devices  11 us (10%)
  Pallas kernels  6.99 us (6%)
  local copies, waits for them, and re-layouts  4.97 us (4%)
  other arithmetic  1.34 us (1%)
    all_to_all x1, blocking collectives, body(): lax.all_to_all(outgoing, 'ep', split_axis=0, concat_axis=0, tiled=True)  47.1 us
    all_to_all x1, waiting for transfers between devices, body(): lax.all_to_all(mine, 'ep', split_axis=0, concat_axis=0, tiled=True)  23.9 us
    all_to_all x1, blocking collectives, body(): lax.all_to_all(blocks, 'tp', split_axis=0, concat_axis=0, tiled=True, axi...  14.9 us
    all_to_all x1, starting transfers between devices, body(): lax.all_to_all(mine, 'ep', split_axis=0, concat_axis=0, tiled=True)  6.64 us
    pallas_call x1, Pallas kernels, body(): pl.pallas_call(other_kernel, out_shape=(both, both), in_specs=[SMEM, VMEM...  3.28 us
    pallas_call x1, Pallas kernels, body(): pl.pallas_call(own_kernel, out_shape=pltpu.VMEM((2, slots_total, units),...  2.6 us
    ppermute x1, starting transfers between devices, body(): theirs = lax.ppermute(send, 'tp', swap)  2.4 us
    unnamed x11, local copies, waits for them, and re-layouts  2.38 us
  transfers between devices with their start and end apart: 3, of which 2 were waited for; matrix products, arithmetic and copies ran while one was open for 1% of the time, Pallas kernels for 2%

profile of v3, /device:TPU:16, one launch (start us, length us, event | category | flops | bytes accessed | tf_op | source)
XLA Modules:
  0.0 112.6 jit_solution(14292369079024610437)
XLA Ops:
  0.0 0.8 copy.23
  0.8 0.1 eq.32.index_ref
  0.9 0.9 copy-done
  1.8 0.7 copy-done.1
  2.5 1.1 dispatch.1
  3.6 47.1 %all_to_all.15 = bf16[64,24,256]{2,1,0:T(8,128)(2,1)S(1)} all-to-all(bf16[64,24,256]{2,1,0:T(8,128)(2,1)S(1)} %bitcast.15), channel_id=1, replica_groups=mesh['ep'=64,'tp'=16] {'ep'}, dimensions={0} | all-to-all | bytes 1572864 | tf_op jit(solution)/shard_map/all_to_all | solution.py:145
  50.7 1.9 %collective-permute-start = (bf16[64,24,256]{2,1,0:T(8,128)(2,1)S(1)}, bf16[64,24,256]{2,1,0:T(8,128)(2,1)S(1)}, u32[]{:S(2)}, u32[]{:S(2)}) collective-permute-start(bf16[64,24,256]{2,1,0:T(8,128)(2,1)S(1)} %all_to_all.15), channel_id=1, source_target_pairs={{0,1},{1,0},{2,3},{3,2},{4,5},{5,4},{6,7},{7,6},{8,9},{9,8},{10,11... | collective-permute-start | bytes 2359304 | tf_op jit(solution)/shard_map/ppermute | solution.py:146
  52.6 0.4 reshape.51.x_ref
  52.9 2.6 %own_half.1.sums_ref = f32[2,192,128]{2,1,0:T(8,128)S(1)} custom-call(s32[1]{0:T(128)} %bitcast.core_ref, bf16[192,2048]{1,0:T(8,128)(2,1)S(1)} %reshape.51.x_ref, bf16[4096,128]{1,0:T(8,128)(2,1)} %bitcast.17, bf16[4096,128]{1,0:T(8,128)(2,1)} %bitcast.19), custom_call_target="tpu_custom_call" | custom-call | tf_op jit(solution)/shard_map/own_half/pallas_call | solution.py:156
  55.6 0.4 reshape.50.x_ref
  55.9 3.3 %other_half.1 = (bf16[192,2048]{1,0:T(8,128)(2,1)S(1)}, bf16[192,2048]{1,0:T(8,128)(2,1)S(1)}) custom-call(s32[1]{0:T(128)} %bitcast.core_ref, bf16[192,2048]{1,0:T(8,128)(2,1)S(1)} %reshape.50.x_ref, f32[2,192,128]{2,1,0:T(8,128)S(1)} %own_half.1.sums_ref, bf16[4096,128]{1,0:T(8,128)(2,1)} %bitcast.18, bf16[4096,128]{1,0:T(8,128)(2,1)} %bitcast.20, ...), custom_call_target="tpu_custom_call" | custom-call | tf_op jit(solution)/shard_map/other_half/pallas_call | solution.py:165
  59.2 2.4 %collective-permute-start.1 = (bf16[192,2048]{1,0:T(8,128)(2,1)S(1)}, bf16[192,2048]{1,0:T(8,128)(2,1)S(1)}, u32[]{:S(2)}, u32[]{:S(2)}) collective-permute-start(bf16[192,2048]{1,0:T(8,128)(2,1)S(1)} %get-tuple-element.8), channel_id=1, source_target_pairs={{0,1},{1,0},{2,3},{3,2},{4,5},{5,4},{6,7},{7,6},{8,9},{9,8},{10,11... | collective-permute-start | bytes 2359304 | tf_op jit(solution)/shard_map/ppermute | solution.py:175
  61.6 1.9 %collective-permute-done.1 = bf16[192,2048]{1,0:T(8,128)(2,1)S(1)} collective-permute-done((bf16[192,2048]{1,0:T(8,128)(2,1)S(1)}, bf16[192,2048]{1,0:T(8,128)(2,1)S(1)}, u32[]{:S(2)}, u32[]{:S(2)}) %collective-permute-start.1) | collective-permute-done | bytes 786464 | tf_op jit(solution)/shard_map/ppermute | solution.py:175
  63.5 0.3 add_convert_fusion
  63.8 1.2 %reshape.52 = bf16[64,24,256]{2,1,0:T(8,128)(2,1)} reshape(bf16[192,2048]{1,0:T(8,128)(2,1)S(1)} %add_convert_fusion) | data formatting | bytes 1572864 | tf_op jit(solution)/shard_map/reshape | solution.py:177
  65.0 6.6 %all-to-all-start.1 = ((bf16[64,24,256]{2,1,0:T(8,128)(2,1)}), bf16[64,24,256]{2,1,0:T(8,128)(2,1)S(1)}, u32[]{:S(2)}, u32[]{:S(2)}) async-start(bf16[64,24,256]{2,1,0:T(8,128)(2,1)} %reshape.52), calls=%async_computation.1 | async-start | bytes 1572864 | tf_op jit(solution)/shard_map/all_to_all | solution.py:178
  71.8 0.1 reduce_window_sum.11
  71.9 0.2 select_reduce_fusion.1
  72.1 0.1 copy.24
  72.4 23.9 %all-to-all-done.1 = bf16[64,24,256]{2,1,0:T(8,128)(2,1)S(1)} async-done(((bf16[64,24,256]{2,1,0:T(8,128)(2,1)}), bf16[64,24,256]{2,1,0:T(8,128)(2,1)S(1)}, u32[]{:S(2)}, u32[]{:S(2)}) %all-to-all-start.1) | async-done | bytes 786464 | tf_op jit(solution)/shard_map/all_to_all | solution.py:178
  96.3 0.4 reshape.53
  96.6 0.4 convolution_convert_fusion
  97.1 14.9 %all_to_all.16 = bf16[8,16,256]{2,1,0:T(8,128)(2,1)S(1)} all-to-all(bf16[8,16,256]{2,1,0:T(8,128)(2,1)S(1)} %bitcast.22), channel_id=1, replica_groups={{0,2,4,6,8,10,12,14},{1,3,5,7,9,11,13,15},{16,18,20,22,24,26,28,30},{17..., dimensions={0} | all-to-all | bytes 131072 | tf_op jit(solution)/shard_map/all_to_all | solution.py:193
  112.0 0.6 reduce_sum.45
  (16 shorter events, 0.3 us)
Async XLA Ops:
  0.9 0.9 copy-start
  1.8 0.7 copy-start.1
  50.7 4.9 %collective-permute-start = (bf16[64,24,256]{2,1,0:T(8,128)(2,1)S(1)}, bf16[64,24,256]{2,1,0:T(8,128)(2,1)S(1)}, u32[]{:S(2)}, u32[]{:S(2)}) collective-permute-start(bf16[64,24,256]{2,1,0:T(8,128)(2,1)S(1)} %all_to_all.15), channel_id=1, source_target_pairs={{0,1},{1,0},{2,3},{3,2},{4,5},{5,4},{6,7},{7,6},{8,9},{9,8},{10,11... | collective-permute-start | bytes 2359304 | tf_op jit(solution)/shard_map/ppermute | solution.py:146
  59.2 4.3 %collective-permute-start.1 = (bf16[192,2048]{1,0:T(8,128)(2,1)S(1)}, bf16[192,2048]{1,0:T(8,128)(2,1)S(1)}, u32[]{:S(2)}, u32[]{:S(2)}) collective-permute-start(bf16[192,2048]{1,0:T(8,128)(2,1)S(1)} %get-tuple-element.8), channel_id=1, source_target_pairs={{0,1},{1,0},{2,3},{3,2},{4,5},{5,4},{6,7},{7,6},{8,9},{9,8},{10,11... | collective-permute-start | bytes 2359304 | tf_op jit(solution)/shard_map/ppermute | solution.py:175
  65.0 7.2 %copy-start.3 = (f32[16,4]{0,1:T(4,128)S(1)}, f32[16,4]{0,1:T(4,128)}, u32[]{:S(2)}) copy-start(f32[16,4]{0,1:T(4,128)} %param.12) | copy-start | bytes 772
  65.0 7.2 %copy-start.4 = (f32[16]{0:T(128)S(1)}, f32[16]{0:T(128)}, u32[]{:S(2)}) copy-start(f32[16]{0:T(128)} %param.11) | copy-start | bytes 196
  65.0 7.2 %copy-start.2 = (s32[16,4]{0,1:T(4,128)S(1)}, s32[16,4]{0,1:T(4,128)}, u32[]{:S(2)}) copy-start(s32[16,4]{0,1:T(4,128)} %param.10) | copy-start | bytes 772
  65.0 31.2 %all-to-all-start.1 = ((bf16[64,24,256]{2,1,0:T(8,128)(2,1)}), bf16[64,24,256]{2,1,0:T(8,128)(2,1)S(1)}, u32[]{:S(2)}, u32[]{:S(2)}) async-start(bf16[64,24,256]{2,1,0:T(8,128)(2,1)} %reshape.52), calls=%async_computation.1 | async-start | bytes 1572864 | tf_op jit(solution)/shard_map/all_to_all | solution.py:178

commit v4 on v2

v4 whole, which is shorter than its diff:
```python
import jax
import jax.numpy as jnp
from jax import lax
from jax.experimental import pallas as pl
from jax.experimental.pallas import tpu as pltpu
from jax.sharding import PartitionSpec as P

GROUPS = 2
BLOCK = 256
LANES = 128


def block_at(b, which):
    return pl.ds(pl.multiple_of((2 * b + which) * BLOCK, BLOCK), BLOCK)


def into_blocks(gate_hbm, up_hbm, which, out_ref, sems):
    return [
        pltpu.make_async_copy(hbm.at[block_at(b, which)], out_ref.at[i, b], sems.at[i, b])
        for b in range(out_ref.shape[1])
        for i, hbm in enumerate((gate_hbm, up_hbm))
    ]


def columns(hbm, which, out_ref, sems):
    return [
        pltpu.make_async_copy(
            hbm.at[:, block_at(b, which)], out_ref.at[:, b * BLOCK : (b + 1) * BLOCK], sems.at[b]
        )
        for b in range(out_ref.shape[1] // BLOCK)
    ]


def dispatch_kernel(
    core_ref, index_ref, tokens_hbm, gain_hbm, gate_hbm, up_hbm, down_hbm,
    out_ref, near_ref, send_ref,
    tokens_ref, gain_ref, count_ref, sems, near_sems, down_sems, *lanes,
):
    core = core_ref[0]
    tokens, width = tokens_ref.shape
    experts, _, chips, share = out_ref.shape
    topk = index_ref.shape[0]
    first = [
        pltpu.make_async_copy(tokens_hbm, tokens_ref, sems.at[0]),
        pltpu.make_async_copy(gain_hbm, gain_ref, sems.at[1]),
    ]
    rest = into_blocks(gate_hbm, up_hbm, core, near_ref, near_sems)
    rest += columns(down_hbm, 1 - core, send_ref, down_sems)
    for copy in first + rest:
        copy.start()
    out_ref[...] = jnp.zeros_like(out_ref)

    def clear(e, _):
        count_ref[e] = 0

    lax.fori_loop(0, experts, clear, None, unroll=8)
    for copy in first:
        copy.wait()
    xf = tokens_ref[...].astype(jnp.float32)
    scale = lax.rsqrt(jnp.mean(xf * xf, axis=-1, keepdims=True) + 1e-06)
    for b in range(chips):
        at = block_at(b, core)
        block = tokens_ref[:, at].astype(jnp.float32) * scale * gain_ref[:, at]
        for i, ref in enumerate(lanes):
            ref[pl.ds(b, tokens, stride=chips), :] = block[:, i * LANES : (i + 1) * LANES]

    def token(t, _):
        here = pl.ds(pl.multiple_of(t * chips, chips), chips)
        row = jnp.concatenate([ref[here, :] for ref in lanes], axis=1).astype(jnp.bfloat16)
        for k in range(topk):
            e = index_ref[k, t]
            rank = count_ref[e]
            count_ref[e] = rank + 1
            out_ref[e, rank] = row

    lax.fori_loop(0, tokens, token, None)
    for copy in rest:
        copy.wait()


def project(x_ref, weights_ref, gate, up):
    for b in range(weights_ref.shape[1]):
        x = x_ref[:, b * BLOCK : (b + 1) * BLOCK]
        gate += jnp.dot(x, weights_ref[0, b], preferred_element_type=jnp.float32)
        up += jnp.dot(x, weights_ref[1, b], preferred_element_type=jnp.float32)
    return gate, up


def own_kernel(
    core_ref, x_ref, near_ref, gate_hbm, up_hbm, down_hbm, sums_ref, far_ref, keep_ref, sems, down_sems
):
    core = core_ref[0]
    copies = into_blocks(gate_hbm, up_hbm, 1 - core, far_ref, sems)
    copies += columns(down_hbm, core, keep_ref, down_sems)
    for copy in copies:
        copy.start()
    zero = jnp.zeros(sums_ref.shape[1:], jnp.float32)
    sums_ref[0], sums_ref[1] = project(x_ref, near_ref, zero, zero)
    for copy in copies:
        copy.wait()


def other_kernel(x_ref, sums_ref, far_ref, hidden_ref):
    gate, up = project(x_ref, far_ref, sums_ref[0], sums_ref[1])
    hidden_ref[...] = (gate * jax.nn.sigmoid(gate) * up).astype(jnp.bfloat16)


def output_kernel(own_ref, theirs_ref, keep_ref, crossed_ref, out_ref, *lanes):
    slots, chips, share = out_ref.shape
    own, theirs = own_ref[...], theirs_ref[...]
    for b in range(chips):
        at = pl.ds(b * BLOCK, BLOCK)
        out = jnp.dot(own, keep_ref[:, at], preferred_element_type=jnp.float32)
        out += jnp.dot(theirs, crossed_ref[:, at], preferred_element_type=jnp.float32)
        for i, ref in enumerate(lanes):
            ref[pl.ds(b, slots, stride=chips), :] = out[:, i * LANES : (i + 1) * LANES]
    for i, ref in enumerate(lanes):
        part = ref[...].reshape(slots, chips, LANES).astype(jnp.bfloat16)
        out_ref[:, :, i * LANES : (i + 1) * LANES] = part


GRANT = pltpu.CompilerParams(vmem_limit_bytes=16 * 2**20)
SMEM = pl.BlockSpec(memory_space=pltpu.SMEM)
VMEM = pl.BlockSpec(memory_space=pltpu.VMEM)
HBM = pl.BlockSpec(memory_space=pltpu.HBM)


def in_vmem(x):
    return pltpu.with_memory_space_constraint(x, pltpu.VMEM)


def in_hbm(x):
    return pltpu.with_memory_space_constraint(x, pltpu.HBM)


def body(tokens, norm_gain, token_expert_index, group_prob, expert_weight, w_gate, w_up, w_down):
    rows_here, width = tokens.shape
    topk = token_expert_index.shape[1]
    experts = lax.axis_size("ep")
    tp_count = lax.axis_size("tp")
    chips = tp_count // 2
    share = width // tp_count
    half = width // 2
    units = w_gate.shape[2]
    core = lax.axis_index("tp") % 2
    swap = [(i, i ^ 1) for i in range(tp_count)]
    same_core = [[2 * i + c for i in range(chips)] for c in range(2)]
    per_group = experts // GROUPS
    capacity = min(rows_here, max(2, rows_here * topk // max(per_group - topk, 1) + 1))
    slots_total = experts * capacity
    gates = group_prob[:, None] * expert_weight / jnp.sum(expert_weight, axis=-1, keepdims=True)
    flattened_index = token_expert_index.reshape(-1)
    onehot = (flattened_index[:, None] == jnp.arange(experts, dtype=jnp.int32)[None, :]).astype(
        jnp.int32
    )
    earlier = jnp.cumsum(onehot, axis=0) - onehot
    slot_rank = jnp.sum(earlier * onehot, axis=1)
    place = flattened_index * capacity + slot_rank
    at_place = jnp.arange(slots_total, dtype=jnp.int32)[:, None] == place[None, :]

    weigh = jnp.sum(
        (at_place.astype(jnp.float32) * gates.reshape(-1)[None, :]).reshape(
            slots_total, rows_here, topk
        ),
        axis=2,
    )

    core_id = core.astype(jnp.int32).reshape(1)
    blocks = pltpu.VMEM((2, chips, share, units), jnp.bfloat16)
    part = pltpu.VMEM((units, half), jnp.bfloat16)
    block_sems = pltpu.SemaphoreType.DMA((2, chips))
    part_sems = pltpu.SemaphoreType.DMA((chips,))
    weights = [in_hbm(w[0]) for w in (w_gate, w_up, w_down)]
    outgoing, near, down_send = pl.pallas_call(
        dispatch_kernel,
        out_shape=(pltpu.VMEM((experts, capacity, chips, share), jnp.bfloat16), blocks, part),
        in_specs=[SMEM, SMEM, HBM, HBM, HBM, HBM, HBM],
        out_specs=(VMEM,) * 3,
        scratch_shapes=[
            pltpu.VMEM((rows_here, width), jnp.bfloat16),
            pltpu.VMEM((1, width), jnp.float32),
            pltpu.SMEM((experts,), jnp.int32),
            pltpu.SemaphoreType.DMA((2,)),
            block_sems,
            part_sems,
            *[pltpu.VMEM((rows_here * chips, LANES), jnp.float32)] * (share // LANES),
        ],
        compiler_params=GRANT,
        name="dispatch",
    )(core_id, token_expert_index.T, in_hbm(tokens), in_hbm(norm_gain[None, :]), *weights)
    outgoing = outgoing.reshape(experts, capacity * chips, share)
    crossed = lax.ppermute(down_send, "tp", swap)
    arrived = lax.all_to_all(outgoing, "ep", split_axis=0, concat_axis=0, tiled=True)
    arrived, crossed, weigh = lax.optimization_barrier((arrived, crossed, weigh))
    arrived = arrived.reshape(slots_total, half)
    other = lax.ppermute(arrived, "tp", swap)
    sums, far, down_keep = pl.pallas_call(
        own_kernel,
        out_shape=(pltpu.VMEM((2, slots_total, units), jnp.float32), blocks, part),
        in_specs=[SMEM, VMEM, VMEM, HBM, HBM, HBM],
        out_specs=(VMEM,) * 3,
        scratch_shapes=[block_sems, part_sems],
        compiler_params=GRANT,
        name="own_half",
    )(core_id, in_vmem(arrived), in_vmem(near), *weights)
    hidden = pl.pallas_call(
        other_kernel,
        out_shape=pltpu.VMEM((slots_total, units), jnp.bfloat16),
        in_specs=[VMEM, VMEM, VMEM],
        out_specs=VMEM,
        compiler_params=GRANT,
        name="other_half",
    )(*(in_vmem(x) for x in (other, sums, far)))
    theirs = lax.ppermute(hidden, "tp", swap)
    mine = pl.pallas_call(
        output_kernel,
        out_shape=pltpu.VMEM((slots_total, chips, share), jnp.bfloat16),
        in_specs=[VMEM, VMEM, VMEM, VMEM],
        out_specs=VMEM,
        scratch_shapes=[pltpu.VMEM((slots_total * chips, LANES), jnp.float32)] * (share // LANES),
        compiler_params=GRANT,
        name="output",
    )(*(in_vmem(x) for x in (hidden, theirs, down_keep, crossed)))
    mine = mine.reshape(experts, capacity * chips, share)
    returned = lax.all_to_all(mine, "ep", split_axis=0, concat_axis=0, tiled=True)
    returned = returned.reshape(slots_total, half)
    partial_mix = jnp.dot(
        weigh.T,
        returned.astype(jnp.float32),
        precision=lax.Precision.HIGHEST,
        preferred_element_type=jnp.float32,
    ).astype(jnp.bfloat16)
    blocks = jnp.moveaxis(partial_mix.reshape(rows_here, chips, share), 1, 0)
    parts = lax.all_to_all(
        blocks, "tp", split_axis=0, concat_axis=0, tiled=True, axis_index_groups=same_core
    )
    return parts.astype(jnp.float32).sum(axis=0).astype(jnp.bfloat16)


def solution(mesh):
    return jax.shard_map(
        body,
        mesh=mesh,
        in_specs=(
            P("ep", None),
            P(),
            P("ep", None),
            P("ep"),
            P("ep", None),
            P("ep", None, "tp"),
            P("ep", None, "tp"),
            P("ep", "tp", None),
        ),
        out_specs=P("ep", "tp"),
        check_vma=False,
    )
```

time: 116 us -> 108 us (0.931)
  Pallas kernels: 0 us -> 6.8 us
  local copies, waits for them, and re-layouts: 9.6 us -> 2.99 us
  waiting for transfers between devices: 25.2 us -> 21.2 us
  other arithmetic: 3.84 us -> 1.08 us
  matrix products: 2.95 us -> 0.42 us
  starting transfers between devices: 27.7 us -> 29.3 us
    pallas_call x0 -> x4, Pallas kernels: none -> 6.8 us  [the longest x1 3.61 us: body(): pl.pallas_call(dispatch_kernel, out_shape=(pltpu.VMEM((experts, capacity,...]
    all_to_all x1, waiting for transfers between devices: 23.3 us -> 20 us  [body(): lax.all_to_all(outgoing, 'ep', split_axis=0, concat_axis=0, tiled=True)]
    reshape x4 -> x0, local copies, waits for them, and re-layouts: 3.13 us -> none  [the longest x1 1.45 us: body(): other = other.reshape(slots_total, half)]
    dot_general x7 -> x0, matrix products: 2.53 us -> none  [the longest x2 0.73 us: out_of(): jnp.dot(hidden, w, preferred_element_type=jnp.float32).astype(jnp.bfloat16)]
    dynamic_slice x3 -> x0, local copies, waits for them, and re-layouts: 2.49 us -> none  [the longest x1 1.09 us: out_of(): w = lax.dynamic_slice_in_dim(down, which, 1, 2).reshape(-1, half)]
    ppermute x1 -> x2, starting transfers between devices: 2.4 us -> 4.05 us  [the longest x1 2.13 us: body(): theirs = lax.ppermute(hidden, 'tp', swap)]
    unnamed x19 -> x7, local copies, waits for them, and re-layouts: 3 us -> 2.02 us
  transfers between devices with their start and end apart: 3 -> 4, of which waited for: 2 -> 3; matrix products, arithmetic and copies ran while one was open for 3% -> 1% of each run, Pallas kernels for 0% -> 2%
where the time goes in v4:
time: 108 us
  blocking collectives  45.7 us (42%)
  starting transfers between devices  29.3 us (27%)
  waiting for transfers between devices  21.2 us (20%)
  Pallas kernels  6.8 us (6%)
  local copies, waits for them, and re-layouts  2.99 us (3%)
  other arithmetic  1.08 us (1%)
    all_to_all x1, blocking collectives, body(): lax.all_to_all(mine, 'ep', split_axis=0, concat_axis=0, tiled=True)  30.8 us
    all_to_all x1, starting transfers between devices, body(): lax.all_to_all(outgoing, 'ep', split_axis=0, concat_axis=0, tiled=True)  23.3 us
    all_to_all x1, waiting for transfers between devices, body(): lax.all_to_all(outgoing, 'ep', split_axis=0, concat_axis=0, tiled=True)  20 us
    all_to_all x1, blocking collectives, body(): lax.all_to_all(blocks, 'tp', split_axis=0, concat_axis=0, tiled=True, axi...  14.9 us
    pallas_call x1, Pallas kernels, body(): pl.pallas_call(dispatch_kernel, out_shape=(pltpu.VMEM((experts, capacity,...  3.61 us
  transfers between devices with their start and end apart: 4, of which 3 were waited for; matrix products, arithmetic and copies ran while one was open for 1% of the time, Pallas kernels for 2%

profile of v4, /device:TPU:16, one launch (start us, length us, event | category | flops | bytes accessed | tf_op | source)
XLA Modules:
  0.0 107.6 jit_solution(17162831769948674042)
XLA Ops:
  0.0 0.7 copy-done
  0.7 3.6 %dispatch.1 = (bf16[64,3,8,256]{3,2,1,0:T(8,128)(2,1)}, bf16[2,8,256,128]{3,2,1,0:T(8,128)(2,1)S(1)}, bf16[128,2048]{1,0:T(8,128)(2,1)S(1)}) custom-call(s32[1]{0:T(128)} %bitcast.core_ref, s32[4,16]{1,0:T(4,128)S(1)} %bitcast.18, bf16[16,4096]{1,0:T(8,128)(2,1)} %tokens_hbm.1, f32[1,4096]{1,0:T(1,128)} %bitcast.27, bf16[4096,128]{1,0:T(8,128)(2,1)} %bitcast.19, ...), custom_call_target="tpu_custom_call" | custom-call | tf_op jit(solution)/shard_map/dispatch/pallas_call | solution.py:174
  4.3 23.3 %all-to-all-start = ((bf16[64,24,256]{2,1,0:T(8,128)(2,1)}), bf16[64,24,256]{2,1,0:T(8,128)(2,1)S(1)}, u32[]{:S(2)}, u32[]{:S(2)}) async-start(bf16[64,24,256]{2,1,0:T(8,128)(2,1)} %bitcast.6), calls=%async_computation | async-start | bytes 1572864 | tf_op jit(solution)/shard_map/all_to_all | solution.py:193
  27.6 1.9 %collective-permute-start = (bf16[128,2048]{1,0:T(8,128)(2,1)S(1)}, bf16[128,2048]{1,0:T(8,128)(2,1)S(1)}, u32[]{:S(2)}, u32[]{:S(2)}) collective-permute-start(bf16[128,2048]{1,0:T(8,128)(2,1)S(1)} %get-tuple-element.15), channel_id=1, source_target_pairs={{0,1},{1,0},{2,3},{3,2},{4,5},{5,4},{6,7},{7,6},{8,9},{9,8},{10,11... | collective-permute-start | bytes 1572872 | tf_op jit(solution)/shard_map/ppermute | solution.py:192
  29.6 0.1 eq.32
  29.8 0.1 reduce_window_sum.11
  29.9 0.2 select_reduce_fusion.1
  30.2 0.6 copy-done.1
  30.9 0.6 copy-done.2
  31.5 0.1 select_reduce_fusion
  31.6 20.0 %all-to-all-done = bf16[64,24,256]{2,1,0:T(8,128)(2,1)S(1)} async-done(((bf16[64,24,256]{2,1,0:T(8,128)(2,1)}), bf16[64,24,256]{2,1,0:T(8,128)(2,1)S(1)}, u32[]{:S(2)}, u32[]{:S(2)}) %all-to-all-start) | async-done | bytes 786464 | tf_op jit(solution)/shard_map/all_to_all | solution.py:193
  51.6 0.4 reshape.47.x_ref
  51.9 1.9 %collective-permute-start.1 = (bf16[192,2048]{1,0:T(8,128)(2,1)S(1)}, bf16[192,2048]{1,0:T(8,128)(2,1)S(1)}, u32[]{:S(2)}, u32[]{:S(2)}) collective-permute-start(bf16[192,2048]{1,0:T(8,128)(2,1)S(1)} %reshape.47.x_ref), channel_id=1, source_target_pairs={{0,1},{1,0},{2,3},{3,2},{4,5},{5,4},{6,7},{7,6},{8,9},{9,8},{10,11... | collective-permute-start | bytes 2359304 | tf_op jit(solution)/shard_map/ppermute | solution.py:196
  53.9 2.0 %own_half.1 = (f32[2,192,128]{2,1,0:T(8,128)S(1)}, bf16[2,8,256,128]{3,2,1,0:T(8,128)(2,1)S(1)}, bf16[128,2048]{1,0:T(8,128)(2,1)S(1)}) custom-call(s32[1]{0:T(128)} %bitcast.core_ref, bf16[192,2048]{1,0:T(8,128)(2,1)S(1)} %reshape.47.x_ref, bf16[2,8,256,128]{3,2,1,0:T(8,128)(2,1)S(1)} %get-tuple-element.18.near_ref, bf16[4096,128]{1,0:T(8,128)(2,1)} %bitcast.20, ...), custom_call_target="tpu_custom_call" | custom-call | tf_op jit(solution)/shard_map/own_half/pallas_call | solution.py:197
  55.8 0.3 collective-permute-done.1.x_ref
  56.1 0.6 other_half.1.own_ref
  56.7 2.1 %collective-permute-start.2 = (bf16[192,128]{1,0:T(8,128)(2,1)S(1)}, bf16[192,128]{1,0:T(8,128)(2,1)S(1)}, u32[]{:S(2)}, u32[]{:S(2)}) collective-permute-start(bf16[192,128]{1,0:T(8,128)(2,1)S(1)} %other_half.1.own_ref), channel_id=1, source_target_pairs={{0,1},{1,0},{2,3},{3,2},{4,5},{5,4},{6,7},{7,6},{8,9},{9,8},{10,11... | collective-permute-start | bytes 147464 | tf_op jit(solution)/shard_map/ppermute | solution.py:214
  58.8 1.0 collective-permute-done.2.theirs_ref
  59.8 0.7 output.1
  60.5 30.8 %all_to_all.15 = bf16[64,24,256]{2,1,0:T(8,128)(2,1)S(1)} all-to-all(bf16[64,24,256]{2,1,0:T(8,128)(2,1)S(1)} %bitcast.17), channel_id=1, replica_groups=mesh['ep'=64,'tp'=16] {'ep'}, dimensions={0} | all-to-all | bytes 1572864 | tf_op jit(solution)/shard_map/all_to_all | solution.py:225
  91.3 0.4 reshape.49
  91.6 0.4 convolution_convert_fusion
  92.1 14.9 %all_to_all.16 = bf16[8,16,256]{2,1,0:T(8,128)(2,1)S(1)} all-to-all(bf16[8,16,256]{2,1,0:T(8,128)(2,1)S(1)} %bitcast.25), channel_id=1, replica_groups={{0,2,4,6,8,10,12,14},{1,3,5,7,9,11,13,15},{16,18,20,22,24,26,28,30},{17..., dimensions={0} | all-to-all | bytes 131072 | tf_op jit(solution)/shard_map/all_to_all | solution.py:234
  107.0 0.6 reduce_sum.45
  (12 shorter events, 0.4 us)
Async XLA Ops:
  0.0 0.7 copy-start
  4.3 47.3 %all-to-all-start = ((bf16[64,24,256]{2,1,0:T(8,128)(2,1)}), bf16[64,24,256]{2,1,0:T(8,128)(2,1)S(1)}, u32[]{:S(2)}, u32[]{:S(2)}) async-start(bf16[64,24,256]{2,1,0:T(8,128)(2,1)} %bitcast.6), calls=%async_computation | async-start | bytes 1572864 | tf_op jit(solution)/shard_map/all_to_all | solution.py:193
  27.6 4.0 %collective-permute-start = (bf16[128,2048]{1,0:T(8,128)(2,1)S(1)}, bf16[128,2048]{1,0:T(8,128)(2,1)S(1)}, u32[]{:S(2)}, u32[]{:S(2)}) collective-permute-start(bf16[128,2048]{1,0:T(8,128)(2,1)S(1)} %get-tuple-element.15), channel_id=1, source_target_pairs={{0,1},{1,0},{2,3},{3,2},{4,5},{5,4},{6,7},{7,6},{8,9},{9,8},{10,11... | collective-permute-start | bytes 1572872 | tf_op jit(solution)/shard_map/ppermute | solution.py:192
  30.1 0.7 copy-start.1
  30.9 0.7 copy-start.2
  51.9 4.2 %collective-permute-start.1 = (bf16[192,2048]{1,0:T(8,128)(2,1)S(1)}, bf16[192,2048]{1,0:T(8,128)(2,1)S(1)}, u32[]{:S(2)}, u32[]{:S(2)}) collective-permute-start(bf16[192,2048]{1,0:T(8,128)(2,1)S(1)} %reshape.47.x_ref), channel_id=1, source_target_pairs={{0,1},{1,0},{2,3},{3,2},{4,5},{5,4},{6,7},{7,6},{8,9},{9,8},{10,11... | collective-permute-start | bytes 2359304 | tf_op jit(solution)/shard_map/ppermute | solution.py:196
  56.7 3.1 %collective-permute-start.2 = (bf16[192,128]{1,0:T(8,128)(2,1)S(1)}, bf16[192,128]{1,0:T(8,128)(2,1)S(1)}, u32[]{:S(2)}, u32[]{:S(2)}) collective-permute-start(bf16[192,128]{1,0:T(8,128)(2,1)S(1)} %other_half.1.own_ref), channel_id=1, source_target_pairs={{0,1},{1,0},{2,3},{3,2},{4,5},{5,4},{6,7},{7,6},{8,9},{9,8},{10,11... | collective-permute-start | bytes 147464 | tf_op jit(solution)/shard_map/ppermute | solution.py:214

commit v5 on v4

v5 whole, which is shorter than its diff:
```python
import jax
import jax.numpy as jnp
from jax import lax
from jax.experimental import pallas as pl
from jax.experimental.pallas import tpu as pltpu
from jax.sharding import PartitionSpec as P

GROUPS = 2
BLOCK = 256
LANES = 128


def block_at(b, which):
    return pl.ds(pl.multiple_of((2 * b + which) * BLOCK, BLOCK), BLOCK)


def into_blocks(gate_hbm, up_hbm, which, out_ref, sems):
    return [
        pltpu.make_async_copy(hbm.at[block_at(b, which)], out_ref.at[i, b], sems.at[i, b])
        for b in range(out_ref.shape[1])
        for i, hbm in enumerate((gate_hbm, up_hbm))
    ]


def columns(hbm, which, out_ref, sems):
    return [
        pltpu.make_async_copy(
            hbm.at[:, block_at(b, which)], out_ref.at[:, b * BLOCK : (b + 1) * BLOCK], sems.at[b]
        )
        for b in range(out_ref.shape[1] // BLOCK)
    ]


def dispatch_kernel(
    index_hbm, tokens_hbm, gain_hbm,
    out_ref,
    index_ref, tokens_ref, gain_ref, count_ref, sems, *lanes,
):
    core = lax.axis_index("tp") % 2
    tokens, width = tokens_ref.shape
    experts, _, chips, share = out_ref.shape
    topk = index_ref.shape[0]
    copies = [
        pltpu.make_async_copy(hbm, ref, sems.at[i])
        for i, (hbm, ref) in enumerate(
            ((tokens_hbm, tokens_ref), (index_hbm, index_ref), (gain_hbm, gain_ref))
        )
    ]
    for copy in copies:
        copy.start()
    out_ref[...] = jnp.zeros_like(out_ref)

    def clear(e, _):
        count_ref[e] = 0

    lax.fori_loop(0, experts, clear, None, unroll=8)
    for copy in copies:
        copy.wait()
    xf = tokens_ref[...].astype(jnp.float32)
    scale = lax.rsqrt(jnp.mean(xf * xf, axis=-1, keepdims=True) + 1e-06)
    for b in range(chips):
        at = block_at(b, core)
        block = tokens_ref[:, at].astype(jnp.float32) * scale * gain_ref[:, at]
        for i, ref in enumerate(lanes):
            ref[pl.ds(b, tokens, stride=chips), :] = block[:, i * LANES : (i + 1) * LANES]

    def token(t, _):
        here = pl.ds(pl.multiple_of(t * chips, chips), chips)
        row = jnp.concatenate([ref[here, :] for ref in lanes], axis=1).astype(jnp.bfloat16)
        for k in range(topk):
            e = index_ref[k, t]
            rank = count_ref[e]
            count_ref[e] = rank + 1
            out_ref[e, rank] = row

    lax.fori_loop(0, tokens, token, None)


def fetch_kernel(
    gate_hbm, up_hbm, down_hbm, near_ref, far_hbm, cross_hbm, near_sems, far_sems, cross_sems
):
    core = lax.axis_index("tp") % 2
    copies = into_blocks(gate_hbm, up_hbm, 1 - core, far_hbm, far_sems)
    copies += columns(down_hbm, 1 - core, cross_hbm, cross_sems)
    copies += into_blocks(gate_hbm, up_hbm, core, near_ref, near_sems)
    for copy in copies:
        copy.start()
    for copy in copies:
        copy.wait()


def sums_kernel(x_ref, near_ref, far_ref, sums_ref, *lanes):
    slots, chips, share = x_ref.shape
    for i, ref in enumerate(lanes):
        part = x_ref[:, :, i * LANES : (i + 1) * LANES].astype(jnp.float32)
        ref[...] = part.reshape(slots * chips, LANES)
    sums = [jnp.zeros(sums_ref.shape[1:], jnp.float32)] * 4
    for b in range(chips):
        rows = pl.ds(b, slots, stride=chips)
        x = jnp.concatenate([ref[rows, :] for ref in lanes], axis=1).astype(jnp.bfloat16)
        for i in range(4):
            w = (near_ref, far_ref)[i // 2][i % 2, b]
            sums[i] += jnp.dot(x, w, preferred_element_type=jnp.float32)
    for i in range(4):
        sums_ref[i] = sums[i]


def down_kernel(down_hbm, crossed_hbm, out_ref, sems, sem):
    units = down_hbm.shape[0]
    copies = columns(down_hbm, lax.axis_index("tp") % 2, out_ref.at[:units], sems)
    copies.append(pltpu.make_async_copy(crossed_hbm, out_ref.at[units:], sem))
    for copy in copies:
        copy.start()
    for copy in copies:
        copy.wait()


def output_kernel(own_ref, theirs_ref, down_ref, out_ref, *lanes):
    slots, chips, share = out_ref.shape
    hidden = []
    for i in (0, 2):
        gate = own_ref[i] + theirs_ref[2 - i]
        up = own_ref[i + 1] + theirs_ref[3 - i]
        hidden.append((gate * jax.nn.sigmoid(gate) * up).astype(jnp.bfloat16))
    hidden = jnp.concatenate(hidden, axis=1)
    for b in range(chips):
        at = pl.ds(b * BLOCK, BLOCK)
        out = jnp.dot(hidden, down_ref[:, at], preferred_element_type=jnp.float32)
        for i, ref in enumerate(lanes):
            ref[pl.ds(b, slots, stride=chips), :] = out[:, i * LANES : (i + 1) * LANES]
    for i, ref in enumerate(lanes):
        part = ref[...].reshape(slots, chips, LANES).astype(jnp.bfloat16)
        out_ref[:, :, i * LANES : (i + 1) * LANES] = part


GRANT = pltpu.CompilerParams(vmem_limit_bytes=16 * 2**20)
VMEM = pl.BlockSpec(memory_space=pltpu.VMEM)
HBM = pl.BlockSpec(memory_space=pltpu.HBM)


def in_vmem(x):
    return pltpu.with_memory_space_constraint(x, pltpu.VMEM)


def in_hbm(x):
    return pltpu.with_memory_space_constraint(x, pltpu.HBM)


def body(tokens, norm_gain, token_expert_index, group_prob, expert_weight, w_gate, w_up, w_down):
    rows_here, width = tokens.shape
    topk = token_expert_index.shape[1]
    experts = lax.axis_size("ep")
    tp_count = lax.axis_size("tp")
    chips = tp_count // 2
    share = width // tp_count
    half = width // 2
    units = w_gate.shape[2]
    swap = [(i, i ^ 1) for i in range(tp_count)]
    same_core = [[2 * i + c for i in range(chips)] for c in range(2)]
    per_group = experts // GROUPS
    capacity = min(rows_here, max(2, rows_here * topk // max(per_group - topk, 1) + 1))
    slots_total = experts * capacity
    gates = group_prob[:, None] * expert_weight / jnp.sum(expert_weight, axis=-1, keepdims=True)
    flattened_index = token_expert_index.reshape(-1)
    onehot = (flattened_index[:, None] == jnp.arange(experts, dtype=jnp.int32)[None, :]).astype(
        jnp.int32
    )
    earlier = jnp.cumsum(onehot, axis=0) - onehot
    slot_rank = jnp.sum(earlier * onehot, axis=1)
    place = flattened_index * capacity + slot_rank
    at_place = jnp.arange(slots_total, dtype=jnp.int32)[:, None] == place[None, :]

    weigh = jnp.sum(
        (at_place.astype(jnp.float32) * gates.reshape(-1)[None, :]).reshape(
            slots_total, rows_here, topk
        ),
        axis=2,
    )

    weights = [in_hbm(w[0]) for w in (w_gate, w_up, w_down)]
    lanes = [pltpu.VMEM((slots_total * chips, LANES), jnp.float32)] * (share // LANES)
    outgoing = pl.pallas_call(
        dispatch_kernel,
        out_shape=jax.ShapeDtypeStruct((experts, capacity, chips, share), jnp.bfloat16),
        in_specs=[HBM, HBM, HBM],
        out_specs=VMEM,
        scratch_shapes=[
            pltpu.SMEM((topk, rows_here), jnp.int32),
            pltpu.VMEM((rows_here, width), jnp.bfloat16),
            pltpu.VMEM((1, width), jnp.float32),
            pltpu.SMEM((experts,), jnp.int32),
            pltpu.SemaphoreType.DMA((3,)),
            *[pltpu.VMEM((rows_here * chips, LANES), jnp.float32)] * (share // LANES),
        ],
        compiler_params=GRANT,
        name="dispatch",
    )(*(in_hbm(x) for x in (token_expert_index.T, tokens, norm_gain[None, :])))
    outgoing = outgoing.reshape(experts, capacity * chips, share)
    near, far, cross = pl.pallas_call(
        fetch_kernel,
        out_shape=(
            pltpu.VMEM((2, chips, share, units), jnp.bfloat16),
            pltpu.HBM((2, chips, share, units), jnp.bfloat16),
            pltpu.HBM((units, half), jnp.bfloat16),
        ),
        in_specs=[HBM, HBM, HBM],
        out_specs=(VMEM, HBM, HBM),
        scratch_shapes=[
            pltpu.SemaphoreType.DMA((2, chips)),
            pltpu.SemaphoreType.DMA((2, chips)),
            pltpu.SemaphoreType.DMA((chips,)),
        ],
        compiler_params=GRANT,
        name="fetch",
    )(*weights)
    far = lax.ppermute(far, "tp", swap)
    cross = lax.ppermute(cross, "tp", swap)
    arrived = lax.all_to_all(outgoing, "ep", split_axis=0, concat_axis=0, tiled=True)
    arrived, near, far, cross, weigh = lax.optimization_barrier((arrived, near, far, cross, weigh))
    sums = pl.pallas_call(
        sums_kernel,
        out_shape=pltpu.VMEM((4, slots_total, units), jnp.float32),
        in_specs=[VMEM, VMEM, VMEM],
        out_specs=VMEM,
        scratch_shapes=lanes,
        compiler_params=GRANT,
        name="sums",
    )(*(in_vmem(x) for x in (arrived.reshape(slots_total, chips, share), near, far)))
    theirs = lax.ppermute(sums, "tp", swap)
    down = pl.pallas_call(
        down_kernel,
        out_shape=pltpu.VMEM((2 * units, half), jnp.bfloat16),
        in_specs=[HBM, HBM],
        out_specs=VMEM,
        scratch_shapes=[pltpu.SemaphoreType.DMA((chips,)), pltpu.SemaphoreType.DMA],
        compiler_params=GRANT,
        name="down",
    )(weights[2], in_hbm(cross))
    mine = pl.pallas_call(
        output_kernel,
        out_shape=pltpu.VMEM((slots_total, chips, share), jnp.bfloat16),
        in_specs=[VMEM, VMEM, VMEM],
        out_specs=VMEM,
        scratch_shapes=lanes,
        compiler_params=GRANT,
        name="output",
    )(*(in_vmem(x) for x in (sums, theirs, down)))
    mine = mine.reshape(experts, capacity * chips, share)
    returned = lax.all_to_all(mine, "ep", split_axis=0, concat_axis=0, tiled=True)
    returned = returned.reshape(slots_total, half)
    partial_mix = jnp.dot(
        weigh.T,
        returned.astype(jnp.float32),
        precision=lax.Precision.HIGHEST,
        preferred_element_type=jnp.float32,
    ).astype(jnp.bfloat16)
    blocks = jnp.moveaxis(partial_mix.reshape(rows_here, chips, share), 1, 0)
    parts = lax.all_to_all(
        blocks, "tp", split_axis=0, concat_axis=0, tiled=True, axis_index_groups=same_core
    )
    return parts.astype(jnp.float32).sum(axis=0).astype(jnp.bfloat16)


def solution(mesh):
    return jax.shard_map(
        body,
        mesh=mesh,
        in_specs=(
            P("ep", None),
            P(),
            P("ep", None),
            P("ep"),
            P("ep", None),
            P("ep", None, "tp"),
            P("ep", None, "tp"),
            P("ep", "tp", None),
        ),
        out_specs=P("ep", "tp"),
        check_vma=False,
    )
```

time: 108 us -> 140 us (1.30)
  Pallas kernels: 6.8 us -> 54.5 us
  waiting for transfers between devices: 21.2 us -> 0.27 us
  blocking collectives: 45.7 us -> 51.9 us
    pallas_call x3 -> x4, Pallas kernels: 6.14 us -> 54 us  [the longest x1 49.1 us: body(): pl.pallas_call(fetch_kernel, out_shape=(pltpu.VMEM((2, chips, share, unit...]
    all_to_all x1, waiting for transfers between devices: 20 us -> 0.01 us  [body(): lax.all_to_all(outgoing, 'ep', split_axis=0, concat_axis=0, tiled=True)]
    all_to_all x1, blocking collectives: 30.8 us -> 37 us  [body(): lax.all_to_all(mine, 'ep', split_axis=0, concat_axis=0, tiled=True)]
  transfers between devices with their start and end apart: 4 -> 4, of which waited for: 3 -> 1; matrix products, arithmetic and copies ran while one was open for 1% -> 1% of each run, Pallas kernels for 2% -> 36%
where the time goes in v5:
time: 140 us
  Pallas kernels  54.5 us (39%)
  blocking collectives  51.9 us (37%)
  starting transfers between devices  29.5 us (21%)
  local copies, waits for them, and re-layouts  1.96 us (1%)
    pallas_call x1, Pallas kernels, body(): pl.pallas_call(fetch_kernel, out_shape=(pltpu.VMEM((2, chips, share, unit...  49.1 us
    all_to_all x1, blocking collectives, body(): lax.all_to_all(mine, 'ep', split_axis=0, concat_axis=0, tiled=True)  37 us
    all_to_all x1, starting transfers between devices, body(): lax.all_to_all(outgoing, 'ep', split_axis=0, concat_axis=0, tiled=True)  23.3 us
    all_to_all x1, blocking collectives, body(): lax.all_to_all(blocks, 'tp', split_axis=0, concat_axis=0, tiled=True, axi...  14.9 us
  transfers between devices with their start and end apart: 4, of which 1 were waited for; matrix products, arithmetic and copies ran while one was open for 1% of the time, Pallas kernels for 36%

profile of v5, /device:TPU:16, one launch (start us, length us, event | category | flops | bytes accessed | tf_op | source)
XLA Modules:
  0.0 139.9 jit_solution(291766353749787255)
XLA Ops:
  0.0 2.3 %dispatch.1 = bf16[64,3,8,256]{3,2,1,0:T(8,128)(2,1)} custom-call(s32[4,16]{1,0:T(4,128)} %bitcast.25, bf16[16,4096]{1,0:T(8,128)(2,1)} %tokens_hbm.1, f32[1,4096]{1,0:T(1,128)} %bitcast.26), custom_call_target="tpu_custom_call" | custom-call | tf_op jit(solution)/shard_map/dispatch/pallas_call | solution.py:182
  2.4 23.3 %all-to-all-start = ((bf16[64,24,256]{2,1,0:T(8,128)(2,1)}), bf16[64,24,256]{2,1,0:T(8,128)(2,1)S(1)}, u32[]{:S(2)}, u32[]{:S(2)}) async-start(bf16[64,24,256]{2,1,0:T(8,128)(2,1)} %bitcast.2), calls=%async_computation | async-start | bytes 1572864 | tf_op jit(solution)/shard_map/all_to_all | solution.py:218
  25.7 49.1 %fetch.1 = (bf16[2,8,256,128]{3,2,1,0:T(8,128)(2,1)S(1)}, bf16[2,8,256,128]{3,2,1,0:T(8,128)(2,1)}, bf16[128,2048]{1,0:T(8,128)(2,1)}) custom-call(bf16[4096,128]{1,0:T(8,128)(2,1)} %bitcast.21, bf16[4096,128]{1,0:T(8,128)(2,1)} %bitcast.22, bf16[128,4096]{1,0:T(8,128)(2,1)} %bitcast.19), custom_call_target="tpu_custom_call" | custom-call | tf_op jit(solution)/shard_map/fetch/pallas_call | solution.py:199
  74.8 1.9 %collective-permute-start = (bf16[2,8,256,128]{3,2,1,0:T(8,128)(2,1)}, bf16[2,8,256,128]{3,2,1,0:T(8,128)(2,1)S(1)}, u32[]{:S(2)}, u32[]{:S(2)}) collective-permute-start(bf16[2,8,256,128]{3,2,1,0:T(8,128)(2,1)} %get-tuple-element.14), channel_id=1, source_target_pairs={{0,1},{1,0},{2,3},{3,2},{4,5},{5,4},{6,7},{7,6},{8,9},{9,8},{10,11... | collective-permute-start | bytes 3145736 | tf_op jit(solution)/shard_map/ppermute | solution.py:216
  76.8 2.4 %collective-permute-start.1 = (bf16[128,2048]{1,0:T(8,128)(2,1)}, bf16[128,2048]{1,0:T(8,128)(2,1)S(1)}, u32[]{:S(2)}, u32[]{:S(2)}) collective-permute-start(bf16[128,2048]{1,0:T(8,128)(2,1)} %get-tuple-element.15), channel_id=1, source_target_pairs={{0,1},{1,0},{2,3},{3,2},{4,5},{5,4},{6,7},{7,6},{8,9},{9,8},{10,11... | collective-permute-start | bytes 1572872 | tf_op jit(solution)/shard_map/ppermute | solution.py:217
  79.2 0.1 copy.23
  79.3 0.1 eq.30
  79.4 0.1 reduce_window_sum.11
  79.5 0.2 select_reduce_fusion.1
  79.7 0.1 reduce_sum.42
  79.8 0.1 copy.24
  79.9 0.6 copy-done.2
  80.5 0.6 copy-done.3
  81.2 0.1 select_reduce_fusion
  81.3 1.1 sums.1.own_ref
  82.4 1.9 %collective-permute-start.2 = (f32[4,192,128]{2,1,0:T(8,128)S(1)}, f32[4,192,128]{2,1,0:T(8,128)S(1)}, u32[]{:S(2)}, u32[]{:S(2)}) collective-permute-start(f32[4,192,128]{2,1,0:T(8,128)S(1)} %sums.1.own_ref), channel_id=1, source_target_pairs={{0,1},{1,0},{2,3},{3,2},{4,5},{5,4},{6,7},{7,6},{8,9},{9,8},{10,11... | collective-permute-start | bytes 1179656 | tf_op jit(solution)/shard_map/ppermute | solution.py:229
  84.3 1.4 %down.1.down_ref = bf16[256,2048]{1,0:T(8,128)(2,1)S(1)} custom-call(bf16[128,4096]{1,0:T(8,128)(2,1)} %bitcast.20, bf16[128,2048]{1,0:T(8,128)(2,1)} %copy-done), custom_call_target="tpu_custom_call" | custom-call | tf_op jit(solution)/shard_map/down/pallas_call | solution.py:230
  85.8 0.3 collective-permute-done.2.theirs_ref
  86.0 0.5 output.1
  86.6 37.0 %all_to_all.15 = bf16[64,24,256]{2,1,0:T(8,128)(2,1)S(1)} all-to-all(bf16[64,24,256]{2,1,0:T(8,128)(2,1)S(1)} %bitcast.18), channel_id=1, replica_groups=mesh['ep'=64,'tp'=16] {'ep'}, dimensions={0} | all-to-all | bytes 1572864 | tf_op jit(solution)/shard_map/all_to_all | solution.py:249
  123.5 0.4 reshape.45
  123.9 0.4 convolution_convert_fusion
  124.3 14.9 %all_to_all.16 = bf16[8,16,256]{2,1,0:T(8,128)(2,1)S(1)} all-to-all(bf16[8,16,256]{2,1,0:T(8,128)(2,1)S(1)} %bitcast.23), channel_id=1, replica_groups={{0,2,4,6,8,10,12,14},{1,3,5,7,9,11,13,15},{16,18,20,22,24,26,28,30},{17..., dimensions={0} | all-to-all | bytes 131072 | tf_op jit(solution)/shard_map/all_to_all | solution.py:258
  139.2 0.6 reduce_sum.45
  (14 shorter events, 0.1 us)
Async XLA Ops:
  2.4 78.9 %all-to-all-start = ((bf16[64,24,256]{2,1,0:T(8,128)(2,1)}), bf16[64,24,256]{2,1,0:T(8,128)(2,1)S(1)}, u32[]{:S(2)}, u32[]{:S(2)}) async-start(bf16[64,24,256]{2,1,0:T(8,128)(2,1)} %bitcast.2), calls=%async_computation | async-start | bytes 1572864 | tf_op jit(solution)/shard_map/all_to_all | solution.py:218
  74.8 4.4 %copy-start.1 = (s32[16,4]{0,1:T(4,128)S(1)}, s32[16,4]{0,1:T(4,128)}, u32[]{:S(2)}) copy-start(s32[16,4]{0,1:T(4,128)} %param.10) | copy-start | bytes 772
  74.8 6.5 %collective-permute-start = (bf16[2,8,256,128]{3,2,1,0:T(8,128)(2,1)}, bf16[2,8,256,128]{3,2,1,0:T(8,128)(2,1)S(1)}, u32[]{:S(2)}, u32[]{:S(2)}) collective-permute-start(bf16[2,8,256,128]{3,2,1,0:T(8,128)(2,1)} %get-tuple-element.14), channel_id=1, source_target_pairs={{0,1},{1,0},{2,3},{3,2},{4,5},{5,4},{6,7},{7,6},{8,9},{9,8},{10,11... | collective-permute-start | bytes 3145736 | tf_op jit(solution)/shard_map/ppermute | solution.py:216
  76.8 4.5 %collective-permute-start.1 = (bf16[128,2048]{1,0:T(8,128)(2,1)}, bf16[128,2048]{1,0:T(8,128)(2,1)S(1)}, u32[]{:S(2)}, u32[]{:S(2)}) collective-permute-start(bf16[128,2048]{1,0:T(8,128)(2,1)} %get-tuple-element.15), channel_id=1, source_target_pairs={{0,1},{1,0},{2,3},{3,2},{4,5},{5,4},{6,7},{7,6},{8,9},{9,8},{10,11... | collective-permute-start | bytes 1572872 | tf_op jit(solution)/shard_map/ppermute | solution.py:217
  79.8 0.7 copy-start.2
  80.5 0.7 copy-start.3
  81.3 1.1 copy-start
  82.4 3.6 %collective-permute-start.2 = (f32[4,192,128]{2,1,0:T(8,128)S(1)}, f32[4,192,128]{2,1,0:T(8,128)S(1)}, u32[]{:S(2)}, u32[]{:S(2)}) collective-permute-start(f32[4,192,128]{2,1,0:T(8,128)S(1)} %sums.1.own_ref), channel_id=1, source_target_pairs={{0,1},{1,0},{2,3},{3,2},{4,5},{5,4},{6,7},{7,6},{8,9},{9,8},{10,11... | collective-permute-start | bytes 1179656 | tf_op jit(solution)/shard_map/ppermute | solution.py:229

commit v6 on v5

--- a/solution.py
+++ b/solution.py
@@ -77,11 +77,11 @@
 
 
 def fetch_kernel(
-    gate_hbm, up_hbm, down_hbm, near_ref, far_hbm, cross_hbm, near_sems, far_sems, cross_sems
+    gate_hbm, up_hbm, down_hbm, near_ref, far_ref, cross_ref, near_sems, far_sems, cross_sems
 ):
     core = lax.axis_index("tp") % 2
-    copies = into_blocks(gate_hbm, up_hbm, 1 - core, far_hbm, far_sems)
-    copies += columns(down_hbm, 1 - core, cross_hbm, cross_sems)
+    copies = into_blocks(gate_hbm, up_hbm, 1 - core, far_ref, far_sems)
+    copies += columns(down_hbm, 1 - core, cross_ref, cross_sems)
     copies += into_blocks(gate_hbm, up_hbm, core, near_ref, near_sems)
     for copy in copies:
         copy.start()
@@ -200,11 +200,11 @@
         fetch_kernel,
         out_shape=(
             pltpu.VMEM((2, chips, share, units), jnp.bfloat16),
-            pltpu.HBM((2, chips, share, units), jnp.bfloat16),
-            pltpu.HBM((units, half), jnp.bfloat16),
+            jax.ShapeDtypeStruct((2, chips, share, units), jnp.bfloat16),
+            jax.ShapeDtypeStruct((units, half), jnp.bfloat16),
         ),
         in_specs=[HBM, HBM, HBM],
-        out_specs=(VMEM, HBM, HBM),
+        out_specs=(VMEM, VMEM, VMEM),
         scratch_shapes=[
             pltpu.SemaphoreType.DMA((2, chips)),
             pltpu.SemaphoreType.DMA((2, chips)),

time: 140 us -> 103 us (0.74)
  Pallas kernels: 54.5 us -> 8.46 us
  waiting for transfers between devices: 0.27 us -> 14.7 us
  blocking collectives: 51.9 us -> 45.7 us
    pallas_call x1, Pallas kernels: 49.1 us -> 3.09 us  [body(): pl.pallas_call(fetch_kernel, out_shape=(pltpu.VMEM((2, chips, share, unit...]
    all_to_all x1, waiting for transfers between devices: 0.01 us -> 14.4 us  [body(): lax.all_to_all(outgoing, 'ep', split_axis=0, concat_axis=0, tiled=True)]
    all_to_all x1, blocking collectives: 37 us -> 30.8 us  [body(): lax.all_to_all(mine, 'ep', split_axis=0, concat_axis=0, tiled=True)]
  transfers between devices with their start and end apart: 4 -> 4, of which waited for: 1 -> 2; matrix products, arithmetic and copies ran while one was open for 1% -> 1% of each run, Pallas kernels for 36% -> 4%
where the time goes in v6:
time: 103 us; the launch traced here: 102 us
  blocking collectives  45.7 us (44%)
  starting transfers between devices  29.5 us (29%)
  waiting for transfers between devices  14.7 us (14%)
  Pallas kernels  8.46 us (8%)
  local copies, waits for them, and re-layouts  1.96 us (2%)
  other arithmetic  1.08 us (1%)
    all_to_all x1, blocking collectives, body(): lax.all_to_all(mine, 'ep', split_axis=0, concat_axis=0, tiled=True)  30.8 us
    all_to_all x1, starting transfers between devices, body(): lax.all_to_all(outgoing, 'ep', split_axis=0, concat_axis=0, tiled=True)  23.3 us
    all_to_all x1, blocking collectives, body(): lax.all_to_all(blocks, 'tp', split_axis=0, concat_axis=0, tiled=True, axi...  14.9 us
    all_to_all x1, waiting for transfers between devices, body(): lax.all_to_all(outgoing, 'ep', split_axis=0, concat_axis=0, tiled=True)  14.4 us
    pallas_call x1, Pallas kernels, body(): pl.pallas_call(fetch_kernel, out_shape=(pltpu.VMEM((2, chips, share, unit...  3.09 us
    ppermute x1, starting transfers between devices, body(): cross = lax.ppermute(cross, 'tp', swap)  2.41 us
    pallas_call x1, Pallas kernels, body(): pl.pallas_call(dispatch_kernel, out_shape=jax.ShapeDtypeStruct((experts,...  2.34 us
  transfers between devices with their start and end apart: 4, of which 2 were waited for; matrix products, arithmetic and copies ran while one was open for 1% of the time, Pallas kernels for 4%

profile of v6, /device:TPU:16, one launch (start us, length us, event | category | flops | bytes accessed | tf_op | source)
XLA Modules:
  0.0 102.0 jit_solution(17142814687082101132)
XLA Ops:
  0.0 2.3 %dispatch.1 = bf16[64,3,8,256]{3,2,1,0:T(8,128)(2,1)} custom-call(s32[4,16]{1,0:T(4,128)} %bitcast.25, bf16[16,4096]{1,0:T(8,128)(2,1)} %tokens_hbm.1, f32[1,4096]{1,0:T(1,128)} %bitcast.26), custom_call_target="tpu_custom_call" | custom-call | tf_op jit(solution)/shard_map/dispatch/pallas_call | solution.py:182
  2.4 23.3 %all-to-all-start = ((bf16[64,24,256]{2,1,0:T(8,128)(2,1)}), bf16[64,24,256]{2,1,0:T(8,128)(2,1)S(1)}, u32[]{:S(2)}, u32[]{:S(2)}) async-start(bf16[64,24,256]{2,1,0:T(8,128)(2,1)} %bitcast.2), calls=%async_computation | async-start | bytes 1572864 | tf_op jit(solution)/shard_map/all_to_all | solution.py:218
  25.7 3.1 %fetch.1 = (bf16[2,8,256,128]{3,2,1,0:T(8,128)(2,1)S(1)}, bf16[2,8,256,128]{3,2,1,0:T(8,128)(2,1)}, bf16[128,2048]{1,0:T(8,128)(2,1)S(1)}) custom-call(bf16[4096,128]{1,0:T(8,128)(2,1)} %bitcast.21, bf16[4096,128]{1,0:T(8,128)(2,1)} %bitcast.22, bf16[128,4096]{1,0:T(8,128)(2,1)} %bitcast.19), custom_call_target="tpu_custom_call" | custom-call | tf_op jit(solution)/shard_map/fetch/pallas_call | solution.py:199
  28.8 1.9 %collective-permute-start = (bf16[2,8,256,128]{3,2,1,0:T(8,128)(2,1)}, bf16[2,8,256,128]{3,2,1,0:T(8,128)(2,1)S(1)}, u32[]{:S(2)}, u32[]{:S(2)}) collective-permute-start(bf16[2,8,256,128]{3,2,1,0:T(8,128)(2,1)} %get-tuple-element.14), channel_id=1, source_target_pairs={{0,1},{1,0},{2,3},{3,2},{4,5},{5,4},{6,7},{7,6},{8,9},{9,8},{10,11... | collective-permute-start | bytes 3145736 | tf_op jit(solution)/shard_map/ppermute | solution.py:216
  30.7 2.4 %collective-permute-start.1 = (bf16[128,2048]{1,0:T(8,128)(2,1)S(1)}, bf16[128,2048]{1,0:T(8,128)(2,1)}, u32[]{:S(2)}, u32[]{:S(2)}) collective-permute-start(bf16[128,2048]{1,0:T(8,128)(2,1)S(1)} %get-tuple-element.15), channel_id=1, source_target_pairs={{0,1},{1,0},{2,3},{3,2},{4,5},{5,4},{6,7},{7,6},{8,9},{9,8},{10,11... | collective-permute-start | bytes 1572872 | tf_op jit(solution)/shard_map/ppermute | solution.py:217
  33.1 0.1 copy.23
  33.2 0.1 eq.30
  33.4 0.1 reduce_window_sum.11
  33.5 0.2 select_reduce_fusion.1
  33.8 0.1 copy.24
  33.8 0.6 copy-done.1
  34.5 0.6 copy-done.2
  35.1 0.1 select_reduce_fusion
  35.2 14.4 %all-to-all-done = bf16[64,24,256]{2,1,0:T(8,128)(2,1)S(1)} async-done(((bf16[64,24,256]{2,1,0:T(8,128)(2,1)}), bf16[64,24,256]{2,1,0:T(8,128)(2,1)S(1)}, u32[]{:S(2)}, u32[]{:S(2)}) %all-to-all-start) | async-done | bytes 786464 | tf_op jit(solution)/shard_map/all_to_all | solution.py:218
  49.6 1.1 %sums.1.own_ref = f32[4,192,128]{2,1,0:T(8,128)S(1)} custom-call(bf16[192,8,256]{2,1,0:T(8,128)(2,1)S(1)} %bitcast.17, bf16[2,8,256,128]{3,2,1,0:T(8,128)(2,1)S(1)} %get-tuple-element.18.near_ref, bf16[2,8,256,128]{3,2,1,0:T(8,128)(2,1)S(1)} %collective-permute-done.far_ref), custom_call_target="tpu_custom_call" | custom-call | tf_op jit(solution)/shard_map/sums/pallas_call | solution.py:220
  50.7 1.9 %collective-permute-start.2 = (f32[4,192,128]{2,1,0:T(8,128)S(1)}, f32[4,192,128]{2,1,0:T(8,128)S(1)}, u32[]{:S(2)}, u32[]{:S(2)}) collective-permute-start(f32[4,192,128]{2,1,0:T(8,128)S(1)} %sums.1.own_ref), channel_id=1, source_target_pairs={{0,1},{1,0},{2,3},{3,2},{4,5},{5,4},{6,7},{7,6},{8,9},{9,8},{10,11... | collective-permute-start | bytes 1179656 | tf_op jit(solution)/shard_map/ppermute | solution.py:229
  52.7 1.4 %down.1.down_ref = bf16[256,2048]{1,0:T(8,128)(2,1)S(1)} custom-call(bf16[128,4096]{1,0:T(8,128)(2,1)} %bitcast.20, bf16[128,2048]{1,0:T(8,128)(2,1)} %collective-permute-done.1.crossed_hbm), custom_call_target="tpu_custom_call" | custom-call | tf_op jit(solution)/shard_map/down/pallas_call | solution.py:230
  54.1 0.3 collective-permute-done.2.theirs_ref
  54.4 0.5 output.1
  54.9 30.8 %all_to_all.15 = bf16[64,24,256]{2,1,0:T(8,128)(2,1)S(1)} all-to-all(bf16[64,24,256]{2,1,0:T(8,128)(2,1)S(1)} %bitcast.18), channel_id=1, replica_groups=mesh['ep'=64,'tp'=16] {'ep'}, dimensions={0} | all-to-all | bytes 1572864 | tf_op jit(solution)/shard_map/all_to_all | solution.py:249
  85.7 0.4 reshape.45
  86.0 0.4 convolution_convert_fusion
  86.5 14.9 %all_to_all.16 = bf16[8,16,256]{2,1,0:T(8,128)(2,1)S(1)} all-to-all(bf16[8,16,256]{2,1,0:T(8,128)(2,1)S(1)} %bitcast.23), channel_id=1, replica_groups={{0,2,4,6,8,10,12,14},{1,3,5,7,9,11,13,15},{16,18,20,22,24,26,28,30},{17..., dimensions={0} | all-to-all | bytes 131072 | tf_op jit(solution)/shard_map/all_to_all | solution.py:258
  101.4 0.6 reduce_sum.45
  (12 shorter events, 0.2 us)
Async XLA Ops:
  2.4 47.3 %all-to-all-start = ((bf16[64,24,256]{2,1,0:T(8,128)(2,1)}), bf16[64,24,256]{2,1,0:T(8,128)(2,1)S(1)}, u32[]{:S(2)}, u32[]{:S(2)}) async-start(bf16[64,24,256]{2,1,0:T(8,128)(2,1)} %bitcast.2), calls=%async_computation | async-start | bytes 1572864 | tf_op jit(solution)/shard_map/all_to_all | solution.py:218
  28.8 4.4 %copy-start = (s32[16,4]{0,1:T(4,128)S(1)}, s32[16,4]{0,1:T(4,128)}, u32[]{:S(2)}) copy-start(s32[16,4]{0,1:T(4,128)} %param.10) | copy-start | bytes 772
  28.8 6.4 %collective-permute-start = (bf16[2,8,256,128]{3,2,1,0:T(8,128)(2,1)}, bf16[2,8,256,128]{3,2,1,0:T(8,128)(2,1)S(1)}, u32[]{:S(2)}, u32[]{:S(2)}) collective-permute-start(bf16[2,8,256,128]{3,2,1,0:T(8,128)(2,1)} %get-tuple-element.14), channel_id=1, source_target_pairs={{0,1},{1,0},{2,3},{3,2},{4,5},{5,4},{6,7},{7,6},{8,9},{9,8},{10,11... | collective-permute-start | bytes 3145736 | tf_op jit(solution)/shard_map/ppermute | solution.py:216
  30.7 4.5 %collective-permute-start.1 = (bf16[128,2048]{1,0:T(8,128)(2,1)S(1)}, bf16[128,2048]{1,0:T(8,128)(2,1)}, u32[]{:S(2)}, u32[]{:S(2)}) collective-permute-start(bf16[128,2048]{1,0:T(8,128)(2,1)S(1)} %get-tuple-element.15), channel_id=1, source_target_pairs={{0,1},{1,0},{2,3},{3,2},{4,5},{5,4},{6,7},{7,6},{8,9},{9,8},{10,11... | collective-permute-start | bytes 1572872 | tf_op jit(solution)/shard_map/ppermute | solution.py:217
  33.7 0.7 copy-start.1
  34.4 0.7 copy-start.2
  50.7 3.6 %collective-permute-start.2 = (f32[4,192,128]{2,1,0:T(8,128)S(1)}, f32[4,192,128]{2,1,0:T(8,128)S(1)}, u32[]{:S(2)}, u32[]{:S(2)}) collective-permute-start(f32[4,192,128]{2,1,0:T(8,128)S(1)} %sums.1.own_ref), channel_id=1, source_target_pairs={{0,1},{1,0},{2,3},{3,2},{4,5},{5,4},{6,7},{7,6},{8,9},{9,8},{10,11... | collective-permute-start | bytes 1179656 | tf_op jit(solution)/shard_map/ppermute | solution.py:229

commit v7 on v6

--- a/solution.py
+++ b/solution.py
@@ -25,10 +25,18 @@
 def columns(hbm, which, out_ref, sems):
     return [
         pltpu.make_async_copy(
-            hbm.at[:, block_at(b, which)], out_ref.at[:, b * BLOCK : (b + 1) * BLOCK], sems.at[b]
+            hbm.at[:, pl.ds(pl.multiple_of((4 * b + which) * BLOCK, BLOCK), BLOCK)],
+            out_ref.at[:, b * BLOCK : (b + 1) * BLOCK],
+            sems.at[b],
         )
         for b in range(out_ref.shape[1] // BLOCK)
     ]
+
+
+def beside(d):
+    here = lax.axis_index("tp") % 4
+    flipped = here + 1 - 2 * (here % 2) if d % 2 else here
+    return (flipped + 2) % 4 if d > 1 else flipped
 
 
 def dispatch_kernel(
@@ -77,11 +85,13 @@
 
 
 def fetch_kernel(
-    gate_hbm, up_hbm, down_hbm, near_ref, far_ref, cross_ref, near_sems, far_sems, cross_sems
+    gate_hbm, up_hbm, down_hbm, near_ref, far_ref, *refs
 ):
     core = lax.axis_index("tp") % 2
+    crosses, (near_sems, far_sems, cross_sems) = refs[:3], refs[3:]
     copies = into_blocks(gate_hbm, up_hbm, 1 - core, far_ref, far_sems)
-    copies += columns(down_hbm, 1 - core, cross_ref, cross_sems)
+    for i, ref in enumerate(crosses):
+        copies += columns(down_hbm, beside(i + 1), ref, cross_sems.at[i])
     copies += into_blocks(gate_hbm, up_hbm, core, near_ref, near_sems)
     for copy in copies:
         copy.start()
@@ -105,32 +115,39 @@
         sums_ref[i] = sums[i]
 
 
-def down_kernel(down_hbm, crossed_hbm, out_ref, sems, sem):
+def down_kernel(down_hbm, *refs):
+    crossed, (out_ref, sems, crossed_sems) = refs[:3], refs[3:]
     units = down_hbm.shape[0]
-    copies = columns(down_hbm, lax.axis_index("tp") % 2, out_ref.at[:units], sems)
-    copies.append(pltpu.make_async_copy(crossed_hbm, out_ref.at[units:], sem))
+    copies = columns(down_hbm, beside(0), out_ref.at[:units], sems)
+    for i, hbm in enumerate(crossed):
+        there = out_ref.at[(i + 1) * units : (i + 2) * units]
+        copies.append(pltpu.make_async_copy(hbm, there, crossed_sems.at[i]))
     for copy in copies:
         copy.start()
     for copy in copies:
         copy.wait()
 
 
-def output_kernel(own_ref, theirs_ref, down_ref, out_ref, *lanes):
-    slots, chips, share = out_ref.shape
+def hidden_kernel(own_ref, theirs_ref, out_ref):
     hidden = []
     for i in (0, 2):
         gate = own_ref[i] + theirs_ref[2 - i]
         up = own_ref[i + 1] + theirs_ref[3 - i]
         hidden.append((gate * jax.nn.sigmoid(gate) * up).astype(jnp.bfloat16))
-    hidden = jnp.concatenate(hidden, axis=1)
-    for b in range(chips):
+    out_ref[...] = jnp.concatenate(hidden, axis=1)
+
+
+def output_kernel(own_ref, theirs_ref, down_ref, out_ref, rows_ref):
+    slots, rows, _ = out_ref.shape
+    hidden = jnp.concatenate([own_ref[...], theirs_ref[...]], axis=1)
+    parts = BLOCK // LANES
+    for b in range(rows // parts):
         at = pl.ds(b * BLOCK, BLOCK)
         out = jnp.dot(hidden, down_ref[:, at], preferred_element_type=jnp.float32)
-        for i, ref in enumerate(lanes):
-            ref[pl.ds(b, slots, stride=chips), :] = out[:, i * LANES : (i + 1) * LANES]
-    for i, ref in enumerate(lanes):
-        part = ref[...].reshape(slots, chips, LANES).astype(jnp.bfloat16)
-        out_ref[:, :, i * LANES : (i + 1) * LANES] = part
+        for i in range(parts):
+            row = pl.ds(b * parts + i, slots, stride=rows)
+            rows_ref[row, :] = out[:, i * LANES : (i + 1) * LANES]
+    out_ref[...] = rows_ref[...].reshape(out_ref.shape).astype(jnp.bfloat16)
 
 
 GRANT = pltpu.CompilerParams(vmem_limit_bytes=16 * 2**20)
@@ -156,7 +173,9 @@
     half = width // 2
     units = w_gate.shape[2]
     swap = [(i, i ^ 1) for i in range(tp_count)]
-    same_core = [[2 * i + c for i in range(chips)] for c in range(2)]
+    across = [[(i, i ^ d) for i in range(tp_count)] for d in (1, 2, 3)]
+    quarter = width // 4
+    every_fourth = [[4 * j + q for j in range(tp_count // 4)] for q in range(4)]
     per_group = experts // GROUPS
     capacity = min(rows_here, max(2, rows_here * topk // max(per_group - topk, 1) + 1))
     slots_total = experts * capacity
@@ -196,27 +215,29 @@
         name="dispatch",
     )(*(in_hbm(x) for x in (token_expert_index.T, tokens, norm_gain[None, :])))
     outgoing = outgoing.reshape(experts, capacity * chips, share)
-    near, far, cross = pl.pallas_call(
+    near, far, *crosses = pl.pallas_call(
         fetch_kernel,
         out_shape=(
             pltpu.VMEM((2, chips, share, units), jnp.bfloat16),
             jax.ShapeDtypeStruct((2, chips, share, units), jnp.bfloat16),
-            jax.ShapeDtypeStruct((units, half), jnp.bfloat16),
+            *[jax.ShapeDtypeStruct((units, quarter), jnp.bfloat16)] * 3,
         ),
         in_specs=[HBM, HBM, HBM],
-        out_specs=(VMEM, VMEM, VMEM),
+        out_specs=(VMEM,) * 5,
         scratch_shapes=[
             pltpu.SemaphoreType.DMA((2, chips)),
             pltpu.SemaphoreType.DMA((2, chips)),
-            pltpu.SemaphoreType.DMA((chips,)),
+            pltpu.SemaphoreType.DMA((3, quarter // BLOCK)),
         ],
         compiler_params=GRANT,
         name="fetch",
     )(*weights)
     far = lax.ppermute(far, "tp", swap)
-    cross = lax.ppermute(cross, "tp", swap)
+    crosses = [lax.ppermute(x, "tp", to) for x, to in zip(crosses, across)]
     arrived = lax.all_to_all(outgoing, "ep", split_axis=0, concat_axis=0, tiled=True)
-    arrived, near, far, cross, weigh = lax.optimization_barrier((arrived, near, far, cross, weigh))
+    arrived, near, far, crosses, weigh = lax.optimization_barrier(
+        (arrived, near, far, crosses, weigh)
+    )
     sums = pl.pallas_call(
         sums_kernel,
         out_shape=pltpu.VMEM((4, slots_total, units), jnp.float32),
@@ -229,34 +250,47 @@
     theirs = lax.ppermute(sums, "tp", swap)
     down = pl.pallas_call(
         down_kernel,
-        out_shape=pltpu.VMEM((2 * units, half), jnp.bfloat16),
-        in_specs=[HBM, HBM],
-        out_specs=VMEM,
-        scratch_shapes=[pltpu.SemaphoreType.DMA((chips,)), pltpu.SemaphoreType.DMA],
+        out_shape=pltpu.VMEM((4 * units, quarter), jnp.bfloat16),
+        in_specs=[HBM] * 4,
+        out_specs=VMEM,
+        scratch_shapes=[
+            pltpu.SemaphoreType.DMA((quarter // BLOCK,)),
+            pltpu.SemaphoreType.DMA((3,)),
+        ],
         compiler_params=GRANT,
         name="down",
-    )(weights[2], in_hbm(cross))
+    )(weights[2], *(in_hbm(x) for x in crosses))
+    hidden = pl.pallas_call(
+        hidden_kernel,
+        out_shape=pltpu.VMEM((slots_total, 2 * units), jnp.bfloat16),
+        in_specs=[VMEM, VMEM],
+        out_specs=VMEM,
+        compiler_params=GRANT,
+        name="hidden",
+    )(in_vmem(sums), in_vmem(theirs))
+    beyond = lax.ppermute(hidden, "tp", across[1])
+    rows = quarter // LANES
     mine = pl.pallas_call(
         output_kernel,
-        out_shape=pltpu.VMEM((slots_total, chips, share), jnp.bfloat16),
+        out_shape=pltpu.VMEM((slots_total, rows, LANES), jnp.bfloat16),
         in_specs=[VMEM, VMEM, VMEM],
         out_specs=VMEM,
-        scratch_shapes=lanes,
+        scratch_shapes=[pltpu.VMEM((slots_total * rows, LANES), jnp.float32)],
         compiler_params=GRANT,
         name="output",
-    )(*(in_vmem(x) for x in (sums, theirs, down)))
-    mine = mine.reshape(experts, capacity * chips, share)
+    )(*(in_vmem(x) for x in (hidden, beyond, down)))
+    mine = mine.reshape(experts, capacity * rows, LANES)
     returned = lax.all_to_all(mine, "ep", split_axis=0, concat_axis=0, tiled=True)
-    returned = returned.reshape(slots_total, half)
+    returned = returned.reshape(slots_total, quarter)
     partial_mix = jnp.dot(
         weigh.T,
         returned.astype(jnp.float32),
         precision=lax.Precision.HIGHEST,
         preferred_element_type=jnp.float32,
     ).astype(jnp.bfloat16)
-    blocks = jnp.moveaxis(partial_mix.reshape(rows_here, chips, share), 1, 0)
+    blocks = jnp.moveaxis(partial_mix.reshape(rows_here, quarter // share, share), 1, 0)
     parts = lax.all_to_all(
-        blocks, "tp", split_axis=0, concat_axis=0, tiled=True, axis_index_groups=same_core
+        blocks, "tp", split_axis=0, concat_axis=0, tiled=True, axis_index_groups=every_fourth
     )
     return parts.astype(jnp.float32).sum(axis=0).astype(jnp.bfloat16)
 

time: 103 us -> 106 us (1.029)
  starting transfers between devices: 29.5 us -> 38.3 us
  blocking collectives: 45.7 us -> 42.7 us
  waiting for transfers between devices: 14.7 us -> 12.5 us
    all_to_all x1, waiting for transfers between devices: 14.4 us -> 1.41 us  [body(): lax.all_to_all(outgoing, 'ep', split_axis=0, concat_axis=0, tiled=True)]
    ppermute x1 -> x4, waiting for transfers between devices: 0.01 us -> 9.42 us  [the longest x3 7.43 us: body(): crosses = [lax.ppermute(x, 'tp', to) for x, to in zip(crosses, across)]]
    ppermute x1 -> x4, starting transfers between devices: 2.41 us -> 11.1 us  [the longest x3 7.73 us: body(): crosses = [lax.ppermute(x, 'tp', to) for x, to in zip(crosses, across)]]
    all_to_all x1, blocking collectives: 30.8 us -> 28.3 us  [body(): lax.all_to_all(mine, 'ep', split_axis=0, concat_axis=0, tiled=True)]
    ppermute x1, waiting for transfers between devices: 0.27 us -> 1.69 us  [body(): theirs = lax.ppermute(sums, 'tp', swap)]
  transfers between devices with their start and end apart: 4 -> 7, of which waited for: 2 -> 5; matrix products, arithmetic and copies ran while one was open for 1% -> 1% of each run, Pallas kernels for 4% -> 4%
where the time goes in v7:
time: 106 us; the launch traced here: 105 us
  blocking collectives  42.7 us (40%)
  starting transfers between devices  38.3 us (36%)
  waiting for transfers between devices  12.5 us (12%)
  Pallas kernels  8.57 us (8%)
  local copies, waits for them, and re-layouts  1.77 us (2%)
  other arithmetic  1.08 us (1%)
    all_to_all x1, blocking collectives, body(): lax.all_to_all(mine, 'ep', split_axis=0, concat_axis=0, tiled=True)  28.3 us
    all_to_all x1, starting transfers between devices, body(): lax.all_to_all(outgoing, 'ep', split_axis=0, concat_axis=0, tiled=True)  23.3 us
    all_to_all x1, blocking collectives, body(): lax.all_to_all(blocks, 'tp', split_axis=0, concat_axis=0, tiled=True, axi...  14.4 us
    ppermute x3, starting transfers between devices, body(): crosses = [lax.ppermute(x, 'tp', to) for x, to in zip(crosses, across)]  7.73 us
    ppermute x3, waiting for transfers between devices, body(): crosses = [lax.ppermute(x, 'tp', to) for x, to in zip(crosses, across)]  7.43 us
    ppermute x1, starting transfers between devices, body(): beyond = lax.ppermute(hidden, 'tp', across[1])  3.4 us
    pallas_call x1, Pallas kernels, body(): pl.pallas_call(fetch_kernel, out_shape=(pltpu.VMEM((2, chips, share, unit...  3.32 us
    pallas_call x1, Pallas kernels, body(): pl.pallas_call(dispatch_kernel, out_shape=jax.ShapeDtypeStruct((experts,...  2.34 us
  transfers between devices with their start and end apart: 7, of which 5 were waited for; matrix products, arithmetic and copies ran while one was open for 1% of the time, Pallas kernels for 4%

profile of v7, /device:TPU:16, one launch (start us, length us, event | category | flops | bytes accessed | tf_op | source)
XLA Modules:
  0.0 105.4 jit_solution(13193925057852013613)
XLA Ops:
  0.0 2.3 %dispatch.1 = bf16[64,3,8,256]{3,2,1,0:T(8,128)(2,1)} custom-call(s32[4,16]{1,0:T(4,128)} %bitcast.25, bf16[16,4096]{1,0:T(8,128)(2,1)} %tokens_hbm.1, f32[1,4096]{1,0:T(1,128)} %bitcast.26), custom_call_target="tpu_custom_call" | custom-call | tf_op jit(solution)/shard_map/dispatch/pallas_call | solution.py:201
  2.4 23.3 %all-to-all-start = ((bf16[64,24,256]{2,1,0:T(8,128)(2,1)}), bf16[64,24,256]{2,1,0:T(8,128)(2,1)S(1)}, u32[]{:S(2)}, u32[]{:S(2)}) async-start(bf16[64,24,256]{2,1,0:T(8,128)(2,1)} %bitcast.2), calls=%async_computation | async-start | bytes 1572864 | tf_op jit(solution)/shard_map/all_to_all | solution.py:237
  25.7 3.3 %fetch.1 = (bf16[2,8,256,128]{3,2,1,0:T(8,128)(2,1)S(1)}, bf16[2,8,256,128]{3,2,1,0:T(8,128)(2,1)}, bf16[128,1024]{1,0:T(8,128)(2,1)}, bf16[128,1024]{1,0:T(8,128)(2,1)S(1)}, bf16[128,1024]{1,0:T(8,128)(2,1)S(1)}) custom-call(bf16[4096,128]{1,0:T(8,128)(2,1)} %bitcast.21, bf16[4096,128]{1,0:T(8,128)(2,1)} %bitcast.22, bf16[128,4096]{1,0:T(8,128)(2,1)} %bitcast.19), custom_call_target="tpu_custom_call" | custom-call | tf_op jit(solution)/shard_map/fetch/pallas_call | solution.py:218
  29.0 1.9 %collective-permute-start = (bf16[2,8,256,128]{3,2,1,0:T(8,128)(2,1)}, bf16[2,8,256,128]{3,2,1,0:T(8,128)(2,1)S(1)}, u32[]{:S(2)}, u32[]{:S(2)}) collective-permute-start(bf16[2,8,256,128]{3,2,1,0:T(8,128)(2,1)} %get-tuple-element.18), channel_id=1, source_target_pairs={{0,1},{1,0},{2,3},{3,2},{4,5},{5,4},{6,7},{7,6},{8,9},{9,8},{10,11... | collective-permute-start | bytes 3145736 | tf_op jit(solution)/shard_map/ppermute | solution.py:235
  30.9 2.4 %collective-permute-start.1 = (bf16[128,1024]{1,0:T(8,128)(2,1)}, bf16[128,1024]{1,0:T(8,128)(2,1)}, u32[]{:S(2)}, u32[]{:S(2)}) collective-permute-start(bf16[128,1024]{1,0:T(8,128)(2,1)} %get-tuple-element.19), channel_id=1, source_target_pairs={{0,1},{1,0},{2,3},{3,2},{4,5},{5,4},{6,7},{7,6},{8,9},{9,8},{10,11... | collective-permute-start | bytes 786440 | tf_op jit(solution)/shard_map/ppermute | solution.py:236
  33.3 3.4 %collective-permute-start.2 = (bf16[128,1024]{1,0:T(8,128)(2,1)S(1)}, bf16[128,1024]{1,0:T(8,128)(2,1)}, u32[]{:S(2)}, u32[]{:S(2)}) collective-permute-start(bf16[128,1024]{1,0:T(8,128)(2,1)S(1)} %get-tuple-element.20), channel_id=1, source_target_pairs={{0,2},{1,3},{2,0},{3,1},{4,6},{5,7},{6,4},{7,5},{8,10},{9,11},{10,... | collective-permute-start | bytes 786440 | tf_op jit(solution)/shard_map/ppermute | solution.py:236
  36.8 1.9 %collective-permute-start.3 = (bf16[128,1024]{1,0:T(8,128)(2,1)S(1)}, bf16[128,1024]{1,0:T(8,128)(2,1)}, u32[]{:S(2)}, u32[]{:S(2)}) collective-permute-start(bf16[128,1024]{1,0:T(8,128)(2,1)S(1)} %get-tuple-element.21), channel_id=1, source_target_pairs={{0,3},{1,2},{2,1},{3,0},{4,7},{5,6},{6,5},{7,4},{8,11},{9,10},{10,... | collective-permute-start | bytes 786440 | tf_op jit(solution)/shard_map/ppermute | solution.py:236
  39.0 0.2 select_reduce_fusion.1
  39.4 0.6 copy-done.1
  40.0 0.6 copy-done.2
  40.8 3.7 %collective-permute-done.2.refs_1_ = bf16[128,1024]{1,0:T(8,128)(2,1)} collective-permute-done((bf16[128,1024]{1,0:T(8,128)(2,1)S(1)}, bf16[128,1024]{1,0:T(8,128)(2,1)}, u32[]{:S(2)}, u32[]{:S(2)}) %collective-permute-start.2) | collective-permute-done | bytes 262176 | tf_op jit(solution)/shard_map/ppermute | solution.py:236
  44.5 3.7 %collective-permute-done.3.refs_2_ = bf16[128,1024]{1,0:T(8,128)(2,1)} collective-permute-done((bf16[128,1024]{1,0:T(8,128)(2,1)S(1)}, bf16[128,1024]{1,0:T(8,128)(2,1)}, u32[]{:S(2)}, u32[]{:S(2)}) %collective-permute-start.3) | collective-permute-done | bytes 262176 | tf_op jit(solution)/shard_map/ppermute | solution.py:236
  48.2 1.4 %all-to-all-done = bf16[64,24,256]{2,1,0:T(8,128)(2,1)S(1)} async-done(((bf16[64,24,256]{2,1,0:T(8,128)(2,1)}), bf16[64,24,256]{2,1,0:T(8,128)(2,1)S(1)}, u32[]{:S(2)}, u32[]{:S(2)}) %all-to-all-start) | async-done | bytes 786464 | tf_op jit(solution)/shard_map/all_to_all | solution.py:237
  49.6 1.1 %sums.1.own_ref = f32[4,192,128]{2,1,0:T(8,128)S(1)} custom-call(bf16[192,8,256]{2,1,0:T(8,128)(2,1)S(1)} %bitcast.17, bf16[2,8,256,128]{3,2,1,0:T(8,128)(2,1)S(1)} %get-tuple-element.24.near_ref, bf16[2,8,256,128]{3,2,1,0:T(8,128)(2,1)S(1)} %collective-permute-done.far_ref), custom_call_target="tpu_custom_call" | custom-call | tf_op jit(solution)/shard_map/sums/pallas_call | solution.py:241
  50.7 1.9 %collective-permute-start.4 = (f32[4,192,128]{2,1,0:T(8,128)S(1)}, f32[4,192,128]{2,1,0:T(8,128)S(1)}, u32[]{:S(2)}, u32[]{:S(2)}) collective-permute-start(f32[4,192,128]{2,1,0:T(8,128)S(1)} %sums.1.own_ref), channel_id=1, source_target_pairs={{0,1},{1,0},{2,3},{3,2},{4,5},{5,4},{6,7},{7,6},{8,9},{9,8},{10,11... | collective-permute-start | bytes 1179656 | tf_op jit(solution)/shard_map/ppermute | solution.py:250
  52.7 1.7 %collective-permute-done.4.theirs_ref = f32[4,192,128]{2,1,0:T(8,128)S(1)} collective-permute-done((f32[4,192,128]{2,1,0:T(8,128)S(1)}, f32[4,192,128]{2,1,0:T(8,128)S(1)}, u32[]{:S(2)}, u32[]{:S(2)}) %collective-permute-start.4) | collective-permute-done | bytes 393248 | tf_op jit(solution)/shard_map/ppermute | solution.py:250
  54.4 3.4 %collective-permute-start.5 = (bf16[192,256]{1,0:T(8,128)(2,1)S(1)}, bf16[192,256]{1,0:T(8,128)(2,1)S(1)}, u32[]{:S(2)}, u32[]{:S(2)}) collective-permute-start(bf16[192,256]{1,0:T(8,128)(2,1)S(1)} %hidden.1.own_ref), channel_id=1, source_target_pairs={{0,2},{1,3},{2,0},{3,1},{4,6},{5,7},{6,4},{7,5},{8,10},{9,11},{10,... | collective-permute-start | bytes 294920 | tf_op jit(solution)/shard_map/ppermute | solution.py:271
  57.8 1.3 %down.1.down_ref = bf16[512,1024]{1,0:T(8,128)(2,1)S(1)} custom-call(bf16[128,4096]{1,0:T(8,128)(2,1)} %bitcast.20, bf16[128,1024]{1,0:T(8,128)(2,1)} %collective-permute-done.1.refs_0_, bf16[128,1024]{1,0:T(8,128)(2,1)} %collective-permute-done.2.refs_1_, bf16[128,1024]{1,0:T(8,128)(2,1)} %collective-permute-done.3.refs_2_), custom_call_target="tpu_custom_call" | custom-call | tf_op jit(solution)/shard_map/down/pallas_call | solution.py:251
  59.2 2.0 %collective-permute-done.5.theirs_ref = bf16[192,256]{1,0:T(8,128)(2,1)S(1)} collective-permute-done((bf16[192,256]{1,0:T(8,128)(2,1)S(1)}, bf16[192,256]{1,0:T(8,128)(2,1)S(1)}, u32[]{:S(2)}, u32[]{:S(2)}) %collective-permute-start.5) | collective-permute-done | bytes 98336 | tf_op jit(solution)/shard_map/ppermute | solution.py:271
  61.1 0.4 output.1
  61.6 28.3 %all_to_all.15 = bf16[64,24,128]{2,1,0:T(8,128)(2,1)S(1)} all-to-all(bf16[64,24,128]{2,1,0:T(8,128)(2,1)S(1)} %bitcast.18), channel_id=1, replica_groups=mesh['ep'=64,'tp'=16] {'ep'}, dimensions={0} | all-to-all | bytes 786432 | tf_op jit(solution)/shard_map/all_to_all | solution.py:283
  90.1 0.3 convolution_convert_fusion
  90.4 14.4 %all_to_all.16 = bf16[4,16,256]{2,1,0:T(8,128)(2,1)S(1)} all-to-all(bf16[4,16,256]{2,1,0:T(8,128)(2,1)S(1)} %bitcast.24), channel_id=1, replica_groups={{0,4,8,12},{1,5,9,13},{2,6,10,14},{3,7,11,15},{16,20,24,28},{17,21,25,2..., dimensions={0} | all-to-all | bytes 65536 | tf_op jit(solution)/shard_map/all_to_all | solution.py:292
  104.8 0.6 reduce_sum.45
  (19 shorter events, 0.9 us)
Async XLA Ops:
  2.4 47.3 %all-to-all-start = ((bf16[64,24,256]{2,1,0:T(8,128)(2,1)}), bf16[64,24,256]{2,1,0:T(8,128)(2,1)S(1)}, u32[]{:S(2)}, u32[]{:S(2)}) async-start(bf16[64,24,256]{2,1,0:T(8,128)(2,1)} %bitcast.2), calls=%async_computation | async-start | bytes 1572864 | tf_op jit(solution)/shard_map/all_to_all | solution.py:237
  29.0 19.2 %collective-permute-start = (bf16[2,8,256,128]{3,2,1,0:T(8,128)(2,1)}, bf16[2,8,256,128]{3,2,1,0:T(8,128)(2,1)S(1)}, u32[]{:S(2)}, u32[]{:S(2)}) collective-permute-start(bf16[2,8,256,128]{3,2,1,0:T(8,128)(2,1)} %get-tuple-element.18), channel_id=1, source_target_pairs={{0,1},{1,0},{2,3},{3,2},{4,5},{5,4},{6,7},{7,6},{8,9},{9,8},{10,11... | collective-permute-start | bytes 3145736 | tf_op jit(solution)/shard_map/ppermute | solution.py:235
  30.9 7.8 %copy-start = (s32[16,4]{0,1:T(4,128)S(1)}, s32[16,4]{0,1:T(4,128)}, u32[]{:S(2)}) copy-start(s32[16,4]{0,1:T(4,128)} %param.10) | copy-start | bytes 772
  30.9 9.9 %collective-permute-start.1 = (bf16[128,1024]{1,0:T(8,128)(2,1)}, bf16[128,1024]{1,0:T(8,128)(2,1)}, u32[]{:S(2)}, u32[]{:S(2)}) collective-permute-start(bf16[128,1024]{1,0:T(8,128)(2,1)} %get-tuple-element.19), channel_id=1, source_target_pairs={{0,1},{1,0},{2,3},{3,2},{4,5},{5,4},{6,7},{7,6},{8,9},{9,8},{10,11... | collective-permute-start | bytes 786440 | tf_op jit(solution)/shard_map/ppermute | solution.py:236
  33.3 11.2 %collective-permute-start.2 = (bf16[128,1024]{1,0:T(8,128)(2,1)S(1)}, bf16[128,1024]{1,0:T(8,128)(2,1)}, u32[]{:S(2)}, u32[]{:S(2)}) collective-permute-start(bf16[128,1024]{1,0:T(8,128)(2,1)S(1)} %get-tuple-element.20), channel_id=1, source_target_pairs={{0,2},{1,3},{2,0},{3,1},{4,6},{5,7},{6,4},{7,5},{8,10},{9,11},{10,... | collective-permute-start | bytes 786440 | tf_op jit(solution)/shard_map/ppermute | solution.py:236
  36.8 11.5 %collective-permute-start.3 = (bf16[128,1024]{1,0:T(8,128)(2,1)S(1)}, bf16[128,1024]{1,0:T(8,128)(2,1)}, u32[]{:S(2)}, u32[]{:S(2)}) collective-permute-start(bf16[128,1024]{1,0:T(8,128)(2,1)S(1)} %get-tuple-element.21), channel_id=1, source_target_pairs={{0,3},{1,2},{2,1},{3,0},{4,7},{5,6},{6,5},{7,4},{8,11},{9,10},{10,... | collective-permute-start | bytes 786440 | tf_op jit(solution)/shard_map/ppermute | solution.py:236
  39.3 0.7 copy-start.1
  40.0 0.7 copy-start.2
  50.7 3.6 %collective-permute-start.4 = (f32[4,192,128]{2,1,0:T(8,128)S(1)}, f32[4,192,128]{2,1,0:T(8,128)S(1)}, u32[]{:S(2)}, u32[]{:S(2)}) collective-permute-start(f32[4,192,128]{2,1,0:T(8,128)S(1)} %sums.1.own_ref), channel_id=1, source_target_pairs={{0,1},{1,0},{2,3},{3,2},{4,5},{5,4},{6,7},{7,6},{8,9},{9,8},{10,11... | collective-permute-start | bytes 1179656 | tf_op jit(solution)/shard_map/ppermute | solution.py:250
  54.4 6.7 %collective-permute-start.5 = (bf16[192,256]{1,0:T(8,128)(2,1)S(1)}, bf16[192,256]{1,0:T(8,128)(2,1)S(1)}, u32[]{:S(2)}, u32[]{:S(2)}) collective-permute-start(bf16[192,256]{1,0:T(8,128)(2,1)S(1)} %hidden.1.own_ref), channel_id=1, source_target_pairs={{0,2},{1,3},{2,0},{3,1},{4,6},{5,7},{6,4},{7,5},{8,10},{9,11},{10,... | collective-permute-start | bytes 294920 | tf_op jit(solution)/shard_map/ppermute | solution.py:271

commit v8 on v6

--- a/solution.py
+++ b/solution.py
@@ -73,7 +73,7 @@
             count_ref[e] = rank + 1
             out_ref[e, rank] = row
 
-    lax.fori_loop(0, tokens, token, None)
+    lax.fori_loop(0, tokens, token, None, unroll=True)
 
 
 def fetch_kernel(
@@ -115,22 +115,22 @@
         copy.wait()
 
 
-def output_kernel(own_ref, theirs_ref, down_ref, out_ref, *lanes):
-    slots, chips, share = out_ref.shape
+def output_kernel(own_ref, theirs_ref, down_ref, out_ref, rows_ref):
+    slots, rows, _ = out_ref.shape
     hidden = []
     for i in (0, 2):
         gate = own_ref[i] + theirs_ref[2 - i]
         up = own_ref[i + 1] + theirs_ref[3 - i]
         hidden.append((gate * jax.nn.sigmoid(gate) * up).astype(jnp.bfloat16))
     hidden = jnp.concatenate(hidden, axis=1)
-    for b in range(chips):
+    parts = BLOCK // LANES
+    for b in range(rows // parts):
         at = pl.ds(b * BLOCK, BLOCK)
         out = jnp.dot(hidden, down_ref[:, at], preferred_element_type=jnp.float32)
-        for i, ref in enumerate(lanes):
-            ref[pl.ds(b, slots, stride=chips), :] = out[:, i * LANES : (i + 1) * LANES]
-    for i, ref in enumerate(lanes):
-        part = ref[...].reshape(slots, chips, LANES).astype(jnp.bfloat16)
-        out_ref[:, :, i * LANES : (i + 1) * LANES] = part
+        for i in range(parts):
+            row = pl.ds(b * parts + i, slots, stride=rows)
+            rows_ref[row, :] = out[:, i * LANES : (i + 1) * LANES]
+    out_ref[...] = rows_ref[...].reshape(out_ref.shape).astype(jnp.bfloat16)
 
 
 GRANT = pltpu.CompilerParams(vmem_limit_bytes=16 * 2**20)
@@ -236,16 +236,17 @@
         compiler_params=GRANT,
         name="down",
     )(weights[2], in_hbm(cross))
+    rows = half // LANES
     mine = pl.pallas_call(
         output_kernel,
-        out_shape=pltpu.VMEM((slots_total, chips, share), jnp.bfloat16),
+        out_shape=pltpu.VMEM((slots_total, rows, LANES), jnp.bfloat16),
         in_specs=[VMEM, VMEM, VMEM],
         out_specs=VMEM,
-        scratch_shapes=lanes,
+        scratch_shapes=[pltpu.VMEM((slots_total * rows, LANES), jnp.float32)],
         compiler_params=GRANT,
         name="output",
     )(*(in_vmem(x) for x in (sums, theirs, down)))
-    mine = mine.reshape(experts, capacity * chips, share)
+    mine = mine.reshape(experts, capacity * rows, LANES)
     returned = lax.all_to_all(mine, "ep", split_axis=0, concat_axis=0, tiled=True)
     returned = returned.reshape(slots_total, half)
     partial_mix = jnp.dot(

time: 103 us -> 103 us (level)
  no operation moved by 1% of the time
where the time goes in v8:
time: 103 us; the launch traced here: 102 us
  blocking collectives  45.7 us (44%)
  starting transfers between devices  29.5 us (29%)
  waiting for transfers between devices  14.7 us (14%)
  Pallas kernels  8.46 us (8%)
  local copies, waits for them, and re-layouts  1.93 us (2%)
  other arithmetic  1.08 us (1%)
    all_to_all x1, blocking collectives, body(): lax.all_to_all(mine, 'ep', split_axis=0, concat_axis=0, tiled=True)  30.8 us
    all_to_all x1, starting transfers between devices, body(): lax.all_to_all(outgoing, 'ep', split_axis=0, concat_axis=0, tiled=True)  23.3 us
    all_to_all x1, blocking collectives, body(): lax.all_to_all(blocks, 'tp', split_axis=0, concat_axis=0, tiled=True, axi...  14.9 us
    all_to_all x1, waiting for transfers between devices, body(): lax.all_to_all(outgoing, 'ep', split_axis=0, concat_axis=0, tiled=True)  14.4 us
    pallas_call x1, Pallas kernels, body(): pl.pallas_call(fetch_kernel, out_shape=(pltpu.VMEM((2, chips, share, unit...  3.09 us
    ppermute x1, starting transfers between devices, body(): cross = lax.ppermute(cross, 'tp', swap)  2.41 us
    pallas_call x1, Pallas kernels, body(): pl.pallas_call(dispatch_kernel, out_shape=jax.ShapeDtypeStruct((experts,...  2.19 us
  transfers between devices with their start and end apart: 4, of which 2 were waited for; matrix products, arithmetic and copies ran while one was open for 1% of the time, Pallas kernels for 4%

profile of v8, /device:TPU:16, one launch (start us, length us, event | category | flops | bytes accessed | tf_op | source)
XLA Modules:
  0.0 102.0 jit_solution(17589771212224034544)
XLA Ops:
  0.0 2.2 %dispatch.1 = bf16[64,3,8,256]{3,2,1,0:T(8,128)(2,1)} custom-call(s32[4,16]{1,0:T(4,128)} %bitcast.25, bf16[16,4096]{1,0:T(8,128)(2,1)} %tokens_hbm.1, f32[1,4096]{1,0:T(1,128)} %bitcast.26), custom_call_target="tpu_custom_call" | custom-call | tf_op jit(solution)/shard_map/dispatch/pallas_call | solution.py:182
  2.2 23.3 %all-to-all-start = ((bf16[64,24,256]{2,1,0:T(8,128)(2,1)}), bf16[64,24,256]{2,1,0:T(8,128)(2,1)S(1)}, u32[]{:S(2)}, u32[]{:S(2)}) async-start(bf16[64,24,256]{2,1,0:T(8,128)(2,1)} %bitcast.2), calls=%async_computation | async-start | bytes 1572864 | tf_op jit(solution)/shard_map/all_to_all | solution.py:218
  25.5 3.1 %fetch.1 = (bf16[2,8,256,128]{3,2,1,0:T(8,128)(2,1)S(1)}, bf16[2,8,256,128]{3,2,1,0:T(8,128)(2,1)}, bf16[128,2048]{1,0:T(8,128)(2,1)S(1)}) custom-call(bf16[4096,128]{1,0:T(8,128)(2,1)} %bitcast.21, bf16[4096,128]{1,0:T(8,128)(2,1)} %bitcast.22, bf16[128,4096]{1,0:T(8,128)(2,1)} %bitcast.19), custom_call_target="tpu_custom_call" | custom-call | tf_op jit(solution)/shard_map/fetch/pallas_call | solution.py:199
  28.6 1.9 %collective-permute-start = (bf16[2,8,256,128]{3,2,1,0:T(8,128)(2,1)}, bf16[2,8,256,128]{3,2,1,0:T(8,128)(2,1)S(1)}, u32[]{:S(2)}, u32[]{:S(2)}) collective-permute-start(bf16[2,8,256,128]{3,2,1,0:T(8,128)(2,1)} %get-tuple-element.14), channel_id=1, source_target_pairs={{0,1},{1,0},{2,3},{3,2},{4,5},{5,4},{6,7},{7,6},{8,9},{9,8},{10,11... | collective-permute-start | bytes 3145736 | tf_op jit(solution)/shard_map/ppermute | solution.py:216
  30.5 2.4 %collective-permute-start.1 = (bf16[128,2048]{1,0:T(8,128)(2,1)S(1)}, bf16[128,2048]{1,0:T(8,128)(2,1)}, u32[]{:S(2)}, u32[]{:S(2)}) collective-permute-start(bf16[128,2048]{1,0:T(8,128)(2,1)S(1)} %get-tuple-element.15), channel_id=1, source_target_pairs={{0,1},{1,0},{2,3},{3,2},{4,5},{5,4},{6,7},{7,6},{8,9},{9,8},{10,11... | collective-permute-start | bytes 1572872 | tf_op jit(solution)/shard_map/ppermute | solution.py:217
  33.0 0.1 copy.23
  33.0 0.1 eq.30
  33.2 0.1 reduce_window_sum.11
  33.3 0.2 select_reduce_fusion.1
  33.6 0.1 copy.24
  33.7 0.6 copy-done.1
  34.3 0.6 copy-done.2
  34.9 0.1 select_reduce_fusion
  35.1 14.4 %all-to-all-done = bf16[64,24,256]{2,1,0:T(8,128)(2,1)S(1)} async-done(((bf16[64,24,256]{2,1,0:T(8,128)(2,1)}), bf16[64,24,256]{2,1,0:T(8,128)(2,1)S(1)}, u32[]{:S(2)}, u32[]{:S(2)}) %all-to-all-start) | async-done | bytes 786464 | tf_op jit(solution)/shard_map/all_to_all | solution.py:218
  49.5 1.1 %sums.1.own_ref = f32[4,192,128]{2,1,0:T(8,128)S(1)} custom-call(bf16[192,8,256]{2,1,0:T(8,128)(2,1)S(1)} %bitcast.17, bf16[2,8,256,128]{3,2,1,0:T(8,128)(2,1)S(1)} %get-tuple-element.18.near_ref, bf16[2,8,256,128]{3,2,1,0:T(8,128)(2,1)S(1)} %collective-permute-done.far_ref), custom_call_target="tpu_custom_call" | custom-call | tf_op jit(solution)/shard_map/sums/pallas_call | solution.py:220
  50.6 1.9 %collective-permute-start.2 = (f32[4,192,128]{2,1,0:T(8,128)S(1)}, f32[4,192,128]{2,1,0:T(8,128)S(1)}, u32[]{:S(2)}, u32[]{:S(2)}) collective-permute-start(f32[4,192,128]{2,1,0:T(8,128)S(1)} %sums.1.own_ref), channel_id=1, source_target_pairs={{0,1},{1,0},{2,3},{3,2},{4,5},{5,4},{6,7},{7,6},{8,9},{9,8},{10,11... | collective-permute-start | bytes 1179656 | tf_op jit(solution)/shard_map/ppermute | solution.py:229
  52.5 1.4 %down.1.down_ref = bf16[256,2048]{1,0:T(8,128)(2,1)S(1)} custom-call(bf16[128,4096]{1,0:T(8,128)(2,1)} %bitcast.20, bf16[128,2048]{1,0:T(8,128)(2,1)} %collective-permute-done.1.crossed_hbm), custom_call_target="tpu_custom_call" | custom-call | tf_op jit(solution)/shard_map/down/pallas_call | solution.py:230
  53.9 0.3 collective-permute-done.2.theirs_ref
  54.2 0.7 output.1
  54.9 30.8 %all_to_all.15 = bf16[64,48,128]{2,1,0:T(8,128)(2,1)S(1)} all-to-all(bf16[64,48,128]{2,1,0:T(8,128)(2,1)S(1)} %bitcast.18), channel_id=1, replica_groups=mesh['ep'=64,'tp'=16] {'ep'}, dimensions={0} | all-to-all | bytes 1572864 | tf_op jit(solution)/shard_map/all_to_all | solution.py:250
  85.7 0.3 reshape.45
  86.0 0.4 convolution_convert_fusion
  86.4 14.9 %all_to_all.16 = bf16[8,16,256]{2,1,0:T(8,128)(2,1)S(1)} all-to-all(bf16[8,16,256]{2,1,0:T(8,128)(2,1)S(1)} %bitcast.23), channel_id=1, replica_groups={{0,2,4,6,8,10,12,14},{1,3,5,7,9,11,13,15},{16,18,20,22,24,26,28,30},{17..., dimensions={0} | all-to-all | bytes 131072 | tf_op jit(solution)/shard_map/all_to_all | solution.py:259
  101.4 0.6 reduce_sum.45
  (12 shorter events, 0.2 us)
Async XLA Ops:
  2.2 47.3 %all-to-all-start = ((bf16[64,24,256]{2,1,0:T(8,128)(2,1)}), bf16[64,24,256]{2,1,0:T(8,128)(2,1)S(1)}, u32[]{:S(2)}, u32[]{:S(2)}) async-start(bf16[64,24,256]{2,1,0:T(8,128)(2,1)} %bitcast.2), calls=%async_computation | async-start | bytes 1572864 | tf_op jit(solution)/shard_map/all_to_all | solution.py:218
  28.6 4.4 %copy-start = (s32[16,4]{0,1:T(4,128)S(1)}, s32[16,4]{0,1:T(4,128)}, u32[]{:S(2)}) copy-start(s32[16,4]{0,1:T(4,128)} %param.10) | copy-start | bytes 772
  28.6 6.4 %collective-permute-start = (bf16[2,8,256,128]{3,2,1,0:T(8,128)(2,1)}, bf16[2,8,256,128]{3,2,1,0:T(8,128)(2,1)S(1)}, u32[]{:S(2)}, u32[]{:S(2)}) collective-permute-start(bf16[2,8,256,128]{3,2,1,0:T(8,128)(2,1)} %get-tuple-element.14), channel_id=1, source_target_pairs={{0,1},{1,0},{2,3},{3,2},{4,5},{5,4},{6,7},{7,6},{8,9},{9,8},{10,11... | collective-permute-start | bytes 3145736 | tf_op jit(solution)/shard_map/ppermute | solution.py:216
  30.5 4.5 %collective-permute-start.1 = (bf16[128,2048]{1,0:T(8,128)(2,1)S(1)}, bf16[128,2048]{1,0:T(8,128)(2,1)}, u32[]{:S(2)}, u32[]{:S(2)}) collective-permute-start(bf16[128,2048]{1,0:T(8,128)(2,1)S(1)} %get-tuple-element.15), channel_id=1, source_target_pairs={{0,1},{1,0},{2,3},{3,2},{4,5},{5,4},{6,7},{7,6},{8,9},{9,8},{10,11... | collective-permute-start | bytes 1572872 | tf_op jit(solution)/shard_map/ppermute | solution.py:217
  33.6 0.7 copy-start.1
  34.3 0.7 copy-start.2
  50.6 3.6 %collective-permute-start.2 = (f32[4,192,128]{2,1,0:T(8,128)S(1)}, f32[4,192,128]{2,1,0:T(8,128)S(1)}, u32[]{:S(2)}, u32[]{:S(2)}) collective-permute-start(f32[4,192,128]{2,1,0:T(8,128)S(1)} %sums.1.own_ref), channel_id=1, source_target_pairs={{0,1},{1,0},{2,3},{3,2},{4,5},{5,4},{6,7},{7,6},{8,9},{9,8},{10,11... | collective-permute-start | bytes 1179656 | tf_op jit(solution)/shard_map/ppermute | solution.py:229

commit v9 on v6

--- a/solution.py
+++ b/solution.py
@@ -73,7 +73,7 @@
             count_ref[e] = rank + 1
             out_ref[e, rank] = row
 
-    lax.fori_loop(0, tokens, token, None)
+    lax.fori_loop(0, tokens, token, None, unroll=True)
 
 
 def fetch_kernel(

time: 103 us -> 102 us (level)
  no operation moved by 1% of the time
where the time goes in v9:
time: 102 us
  blocking collectives  45.7 us (45%)
  starting transfers between devices  29.5 us (29%)
  waiting for transfers between devices  14.7 us (14%)
  Pallas kernels  8.3 us (8%)
  local copies, waits for them, and re-layouts  1.96 us (2%)
  other arithmetic  1.08 us (1%)
    all_to_all x1, blocking collectives, body(): lax.all_to_all(mine, 'ep', split_axis=0, concat_axis=0, tiled=True)  30.8 us
    all_to_all x1, starting transfers between devices, body(): lax.all_to_all(outgoing, 'ep', split_axis=0, concat_axis=0, tiled=True)  23.3 us
    all_to_all x1, blocking collectives, body(): lax.all_to_all(blocks, 'tp', split_axis=0, concat_axis=0, tiled=True, axi...  14.9 us
    all_to_all x1, waiting for transfers between devices, body(): lax.all_to_all(outgoing, 'ep', split_axis=0, concat_axis=0, tiled=True)  14.4 us
    pallas_call x1, Pallas kernels, body(): pl.pallas_call(fetch_kernel, out_shape=(pltpu.VMEM((2, chips, share, unit...  3.09 us
    ppermute x1, starting transfers between devices, body(): cross = lax.ppermute(cross, 'tp', swap)  2.41 us
    pallas_call x1, Pallas kernels, body(): pl.pallas_call(dispatch_kernel, out_shape=jax.ShapeDtypeStruct((experts,...  2.19 us
  transfers between devices with their start and end apart: 4, of which 2 were waited for; matrix products, arithmetic and copies ran while one was open for 1% of the time, Pallas kernels for 4%

profile of v9, /device:TPU:16, one launch (start us, length us, event | category | flops | bytes accessed | tf_op | source)
XLA Modules:
  0.0 101.9 jit_solution(14632354662390451117)
XLA Ops:
  0.0 2.2 %dispatch.1 = bf16[64,3,8,256]{3,2,1,0:T(8,128)(2,1)} custom-call(s32[4,16]{1,0:T(4,128)} %bitcast.25, bf16[16,4096]{1,0:T(8,128)(2,1)} %tokens_hbm.1, f32[1,4096]{1,0:T(1,128)} %bitcast.26), custom_call_target="tpu_custom_call" | custom-call | tf_op jit(solution)/shard_map/dispatch/pallas_call | solution.py:182
  2.2 23.3 %all-to-all-start = ((bf16[64,24,256]{2,1,0:T(8,128)(2,1)}), bf16[64,24,256]{2,1,0:T(8,128)(2,1)S(1)}, u32[]{:S(2)}, u32[]{:S(2)}) async-start(bf16[64,24,256]{2,1,0:T(8,128)(2,1)} %bitcast.2), calls=%async_computation | async-start | bytes 1572864 | tf_op jit(solution)/shard_map/all_to_all | solution.py:218
  25.5 3.1 %fetch.1 = (bf16[2,8,256,128]{3,2,1,0:T(8,128)(2,1)S(1)}, bf16[2,8,256,128]{3,2,1,0:T(8,128)(2,1)}, bf16[128,2048]{1,0:T(8,128)(2,1)S(1)}) custom-call(bf16[4096,128]{1,0:T(8,128)(2,1)} %bitcast.21, bf16[4096,128]{1,0:T(8,128)(2,1)} %bitcast.22, bf16[128,4096]{1,0:T(8,128)(2,1)} %bitcast.19), custom_call_target="tpu_custom_call" | custom-call | tf_op jit(solution)/shard_map/fetch/pallas_call | solution.py:199
  28.6 1.9 %collective-permute-start = (bf16[2,8,256,128]{3,2,1,0:T(8,128)(2,1)}, bf16[2,8,256,128]{3,2,1,0:T(8,128)(2,1)S(1)}, u32[]{:S(2)}, u32[]{:S(2)}) collective-permute-start(bf16[2,8,256,128]{3,2,1,0:T(8,128)(2,1)} %get-tuple-element.14), channel_id=1, source_target_pairs={{0,1},{1,0},{2,3},{3,2},{4,5},{5,4},{6,7},{7,6},{8,9},{9,8},{10,11... | collective-permute-start | bytes 3145736 | tf_op jit(solution)/shard_map/ppermute | solution.py:216
  30.5 2.4 %collective-permute-start.1 = (bf16[128,2048]{1,0:T(8,128)(2,1)S(1)}, bf16[128,2048]{1,0:T(8,128)(2,1)}, u32[]{:S(2)}, u32[]{:S(2)}) collective-permute-start(bf16[128,2048]{1,0:T(8,128)(2,1)S(1)} %get-tuple-element.15), channel_id=1, source_target_pairs={{0,1},{1,0},{2,3},{3,2},{4,5},{5,4},{6,7},{7,6},{8,9},{9,8},{10,11... | collective-permute-start | bytes 1572872 | tf_op jit(solution)/shard_map/ppermute | solution.py:217
  33.0 0.1 copy.23
  33.0 0.1 eq.30
  33.2 0.1 reduce_window_sum.11
  33.3 0.2 select_reduce_fusion.1
  33.6 0.1 copy.24
  33.7 0.6 copy-done.1
  34.3 0.6 copy-done.2
  34.9 0.1 select_reduce_fusion
  35.1 14.4 %all-to-all-done = bf16[64,24,256]{2,1,0:T(8,128)(2,1)S(1)} async-done(((bf16[64,24,256]{2,1,0:T(8,128)(2,1)}), bf16[64,24,256]{2,1,0:T(8,128)(2,1)S(1)}, u32[]{:S(2)}, u32[]{:S(2)}) %all-to-all-start) | async-done | bytes 786464 | tf_op jit(solution)/shard_map/all_to_all | solution.py:218
  49.5 1.1 %sums.1.own_ref = f32[4,192,128]{2,1,0:T(8,128)S(1)} custom-call(bf16[192,8,256]{2,1,0:T(8,128)(2,1)S(1)} %bitcast.17, bf16[2,8,256,128]{3,2,1,0:T(8,128)(2,1)S(1)} %get-tuple-element.18.near_ref, bf16[2,8,256,128]{3,2,1,0:T(8,128)(2,1)S(1)} %collective-permute-done.far_ref), custom_call_target="tpu_custom_call" | custom-call | tf_op jit(solution)/shard_map/sums/pallas_call | solution.py:220
  50.6 1.9 %collective-permute-start.2 = (f32[4,192,128]{2,1,0:T(8,128)S(1)}, f32[4,192,128]{2,1,0:T(8,128)S(1)}, u32[]{:S(2)}, u32[]{:S(2)}) collective-permute-start(f32[4,192,128]{2,1,0:T(8,128)S(1)} %sums.1.own_ref), channel_id=1, source_target_pairs={{0,1},{1,0},{2,3},{3,2},{4,5},{5,4},{6,7},{7,6},{8,9},{9,8},{10,11... | collective-permute-start | bytes 1179656 | tf_op jit(solution)/shard_map/ppermute | solution.py:229
  52.5 1.4 %down.1.down_ref = bf16[256,2048]{1,0:T(8,128)(2,1)S(1)} custom-call(bf16[128,4096]{1,0:T(8,128)(2,1)} %bitcast.20, bf16[128,2048]{1,0:T(8,128)(2,1)} %collective-permute-done.1.crossed_hbm), custom_call_target="tpu_custom_call" | custom-call | tf_op jit(solution)/shard_map/down/pallas_call | solution.py:230
  53.9 0.3 collective-permute-done.2.theirs_ref
  54.2 0.5 output.1
  54.7 30.8 %all_to_all.15 = bf16[64,24,256]{2,1,0:T(8,128)(2,1)S(1)} all-to-all(bf16[64,24,256]{2,1,0:T(8,128)(2,1)S(1)} %bitcast.18), channel_id=1, replica_groups=mesh['ep'=64,'tp'=16] {'ep'}, dimensions={0} | all-to-all | bytes 1572864 | tf_op jit(solution)/shard_map/all_to_all | solution.py:249
  85.5 0.4 reshape.45
  85.9 0.4 convolution_convert_fusion
  86.3 14.9 %all_to_all.16 = bf16[8,16,256]{2,1,0:T(8,128)(2,1)S(1)} all-to-all(bf16[8,16,256]{2,1,0:T(8,128)(2,1)S(1)} %bitcast.23), channel_id=1, replica_groups={{0,2,4,6,8,10,12,14},{1,3,5,7,9,11,13,15},{16,18,20,22,24,26,28,30},{17..., dimensions={0} | all-to-all | bytes 131072 | tf_op jit(solution)/shard_map/all_to_all | solution.py:258
  101.2 0.6 reduce_sum.45
  (12 shorter events, 0.2 us)
Async XLA Ops:
  2.2 47.3 %all-to-all-start = ((bf16[64,24,256]{2,1,0:T(8,128)(2,1)}), bf16[64,24,256]{2,1,0:T(8,128)(2,1)S(1)}, u32[]{:S(2)}, u32[]{:S(2)}) async-start(bf16[64,24,256]{2,1,0:T(8,128)(2,1)} %bitcast.2), calls=%async_computation | async-start | bytes 1572864 | tf_op jit(solution)/shard_map/all_to_all | solution.py:218
  28.6 4.4 %copy-start = (s32[16,4]{0,1:T(4,128)S(1)}, s32[16,4]{0,1:T(4,128)}, u32[]{:S(2)}) copy-start(s32[16,4]{0,1:T(4,128)} %param.10) | copy-start | bytes 772
  28.6 6.4 %collective-permute-start = (bf16[2,8,256,128]{3,2,1,0:T(8,128)(2,1)}, bf16[2,8,256,128]{3,2,1,0:T(8,128)(2,1)S(1)}, u32[]{:S(2)}, u32[]{:S(2)}) collective-permute-start(bf16[2,8,256,128]{3,2,1,0:T(8,128)(2,1)} %get-tuple-element.14), channel_id=1, source_target_pairs={{0,1},{1,0},{2,3},{3,2},{4,5},{5,4},{6,7},{7,6},{8,9},{9,8},{10,11... | collective-permute-start | bytes 3145736 | tf_op jit(solution)/shard_map/ppermute | solution.py:216
  30.5 4.5 %collective-permute-start.1 = (bf16[128,2048]{1,0:T(8,128)(2,1)S(1)}, bf16[128,2048]{1,0:T(8,128)(2,1)}, u32[]{:S(2)}, u32[]{:S(2)}) collective-permute-start(bf16[128,2048]{1,0:T(8,128)(2,1)S(1)} %get-tuple-element.15), channel_id=1, source_target_pairs={{0,1},{1,0},{2,3},{3,2},{4,5},{5,4},{6,7},{7,6},{8,9},{9,8},{10,11... | collective-permute-start | bytes 1572872 | tf_op jit(solution)/shard_map/ppermute | solution.py:217
  33.6 0.7 copy-start.1
  34.3 0.7 copy-start.2
  50.6 3.6 %collective-permute-start.2 = (f32[4,192,128]{2,1,0:T(8,128)S(1)}, f32[4,192,128]{2,1,0:T(8,128)S(1)}, u32[]{:S(2)}, u32[]{:S(2)}) collective-permute-start(f32[4,192,128]{2,1,0:T(8,128)S(1)} %sums.1.own_ref), channel_id=1, source_target_pairs={{0,1},{1,0},{2,3},{3,2},{4,5},{5,4},{6,7},{7,6},{8,9},{9,8},{10,11... | collective-permute-start | bytes 1179656 | tf_op jit(solution)/shard_map/ppermute | solution.py:229
